TPU v7x, 32 devices: a whole 2x2x4 slice. The times are simulated.
32 devices in a mesh: sp: 8 (over z, x), tp: 4 (over y, core).
Axes of the slice: x: 2, y: 2, z: 4, core: 2. Of those that a mesh axis runs over, the one named last changes fastest.
Arguments:
- query_rows: bfloat16 [2048, 2048], P('sp', 'tp'), may hold values from -6 to 6
- key_rows: bfloat16 [2048, 2048], P('sp', 'tp'), may hold values from -6 to 6
- value_rows: bfloat16 [2048, 2048], P('sp', 'tp'), may hold values from -6 to 6
- gate_rows: bfloat16 [2048, 2048], P('sp', 'tp'), may hold values from -6 to 6
- log_decay: float32 [2048, 16], P('sp', 'tp'), may hold values from -1 to 0
- head_gain: float32 [2048], P('tp'), may hold values from 0.1 to 1.9
- out_weight: bfloat16 [2048, 2048], P('tp'), may hold values from -0.125 to 0.125
- residual: bfloat16 [2048, 2048], P(('sp', 'tp')), may hold values from -6 to 6
- ffn_gain: float32 [2048], replicated, may hold values from 0.1 to 1.9
- gate_weight: bfloat16 [8, 2048, 2048], P('sp', None, 'tp'), may hold values from -0.375 to 0.375
- up_weight: bfloat16 [8, 2048, 2048], P('sp', None, 'tp'), may hold values from -0.375 to 0.375
- down_weight: bfloat16 [8, 2048, 2048], P('sp', 'tp'), may hold values from -0.01953125 to 0.01953125
- routes: int32 [2048, 4], P('sp'), may hold values from 0 to 7, all different within a row; in each aligned block of 64 rows (0 to 63, 64 to 127, ...) at most 48 rows name the same one
- route_weights: float32 [2048, 4], P(('sp', 'tp')), may hold values from 0.05 to 1
Outputs:
- layer_out: bfloat16 [2048, 2048], P(('sp', 'tp'))
Inputs may be any that keep to these rules, and one draw needn't show every extreme that they name: `routes`: each row names 4 different experts. In each aligned block of 64 rows no expert is named by more than 48 rows, and in some block some expert is named by exactly 48 rows.
All inputs are finite; a program needn't handle non-finite values.
Results may differ from a plain program's by a relative error of at most 0.014.
Values may be sent and summed in bfloat16 or wider, within the bound.
A program may use at most 128 MiB of HBM per device.

v0:
```python
import functools

import jax
import jax.numpy as jnp
from jax import lax
from jax.experimental import pallas as pl
from jax.experimental.pallas import tpu as pltpu
from jax.sharding import PartitionSpec as P

HEAD_DIM = 128
TOPK = 4
BLOCK = 128


highest = lax.Precision.HIGHEST
rope_base = 10000.0
group_eps = 1e-05
square_eps = 1e-06
clamp_limit = 7.0
swish_alpha = 1.702


def rotary_angles(positions, head_dim):
    half_dim = head_dim // 2
    inverse = rope_base ** (-jnp.arange(half_dim, dtype=jnp.float32) / half_dim)
    return positions[:, None] * inverse[None, :]


def square_norm(updated, gain_row):
    factor = lax.rsqrt(jnp.mean(updated * updated, axis=-1, keepdims=True) + square_eps)
    return (updated * factor * gain_row).astype(jnp.bfloat16)


def expert_rows(rows, gate_part, up_part):
    gate_pre = jnp.dot(rows, gate_part, preferred_element_type=jnp.float32)
    up_pre = jnp.dot(rows, up_part, preferred_element_type=jnp.float32)
    gate_clip = jnp.minimum(gate_pre, clamp_limit)
    up_clip = jnp.clip(up_pre, -clamp_limit, clamp_limit)
    return ((up_clip + 1.0) * (gate_clip * jax.nn.sigmoid(gate_clip * swish_alpha))).astype(
        jnp.bfloat16
    )


def slot_ranks(route_block, experts):
    flat_routes = route_block.reshape(-1)
    onehot = (flat_routes[:, None] == jnp.arange(experts, dtype=jnp.int32)[None, :]).astype(
        jnp.int32
    )
    return (flat_routes, jnp.sum(jnp.cumsum(onehot, axis=0) * onehot, axis=1) - 1)


def retention_kernel(q_ref, k_ref, v_ref, cos_ref, sin_ref, cum_ref, cum_row_ref, ret_ref, qdec_ref, state_ref):
    head = pl.program_id(0)
    length = q_ref.shape[0]
    cosine, sine = cos_ref[...], sin_ref[...]
    half = HEAD_DIM // 2

    def turned(ref):
        rows = ref[...].astype(jnp.float32)
        return rows * cosine + pltpu.roll(rows, half, 1) * sine

    lanes = lax.broadcasted_iota(jnp.int32, cum_ref.shape, 1)
    column = jnp.sum(jnp.where(lanes == head, cum_ref[...], 0.0), axis=1, keepdims=True)
    row = cum_row_ref[0]
    queries = turned(q_ref)
    keys = turned(k_ref) * HEAD_DIM ** (-0.5)
    values = v_ref[...]
    scores = lax.dot_general(
        queries.astype(jnp.bfloat16),
        keys.astype(jnp.bfloat16),
        (((1,), (1,)), ((), ())),
        preferred_element_type=jnp.float32,
    )
    causal = lax.broadcasted_iota(jnp.int32, (length, length), 0) >= lax.broadcasted_iota(
        jnp.int32, (length, length), 1
    )
    weights = jnp.where(causal, jnp.exp(jnp.minimum(column - row, 0.0)), 0.0)
    ret_ref[...] = jnp.dot(
        (scores * weights).astype(jnp.bfloat16), values, preferred_element_type=jnp.float32
    )
    qdec_ref[...] = (queries * jnp.exp(column)).astype(jnp.bfloat16)
    total = column[length - 1 :, :]
    tailed = (keys * jnp.exp(total - column)).astype(jnp.bfloat16)
    state_ref[0, :HEAD_DIM, :] = lax.dot_general(
        tailed, values, (((0,), (0,)), ((), ())), preferred_element_type=jnp.float32
    )
    state_ref[0, HEAD_DIM:, :] = jnp.broadcast_to(total, (8, HEAD_DIM))


def norm_kernel(ret_ref, qdec_ref, enter_ref, gain_ref, gate_ref, hidden_ref):
    retained = ret_ref[...] + jnp.dot(
        qdec_ref[...], enter_ref[0].astype(jnp.bfloat16), preferred_element_type=jnp.float32
    )
    centred = retained - jnp.mean(retained, axis=-1, keepdims=True)
    variance = jnp.mean(centred * centred, axis=-1, keepdims=True)
    gate = gate_ref[...].astype(jnp.float32)
    scaled = centred * lax.rsqrt(variance + group_eps) * gain_ref[...]
    hidden_ref[...] = (scaled * (gate / (1.0 + jnp.exp(-gate)))).astype(jnp.bfloat16)


def greet(devices):
    barrier = pltpu.get_barrier_semaphore()
    for device in devices:
        pl.semaphore_signal(barrier, inc=1, device_id=device, device_id_type=pl.DeviceIdType.MESH)
    pl.semaphore_wait(barrier, len(devices))


def state_kernel(planes, state, totals, entering, gs, gt, ssem, rsem, lsem):
    sp, tp = lax.axis_index("sp"), lax.axis_index("tp")
    z, x = sp // 2, sp % 2
    heads = state.shape[0]
    to_x = {"sp": z * 2 + (1 - x), "tp": tp}

    def later(i):
        return {"sp": ((z + i) % planes) * 2 + x, "tp": tp}

    def plane_of(i):
        return (z + planes - i) % planes

    def move(kind, i, ref, device):
        return pltpu.make_async_remote_copy(
            src_ref=ref, dst_ref=ref, send_sem=ssem.at[kind, i], recv_sem=rsem.at[kind, i],
            device_id=device, device_id_type=pl.DeviceIdType.MESH,
        )

    own = [
        pltpu.make_async_copy(state, gs.at[z, x], lsem.at[0]),
        pltpu.make_async_copy(totals, gt.at[z, x], lsem.at[1]),
    ]
    for copy in own:
        copy.start()
    greet([to_x] + [later(i) for i in range(1, planes)])
    for copy in own:
        copy.wait()
    for i in range(1, planes):
        move(0, i, gs.at[z, x], later(i)).start()
        move(1, i, gt.at[z, x], later(i)).start()
    for i in range(planes):
        p = plane_of(i)
        if i > 0:
            move(0, i, gs.at[p, x], to_x).wait_recv()
            move(1, i, gt.at[p, x], to_x).wait_recv()
        move(2, i, gs.at[p, x], to_x).start()
        move(3, i, gt.at[p, x], to_x).start()
    for i in range(planes):
        p = plane_of(i)
        move(2, i, gs.at[p, 1 - x], to_x).wait_recv()
        move(3, i, gt.at[p, 1 - x], to_x).wait_recv()
    running = jnp.zeros((8, HEAD_DIM), jnp.float32)
    sums = [jnp.zeros((HEAD_DIM, HEAD_DIM), jnp.float32) for _ in range(heads)]
    for s in reversed(range(2 * planes)):
        earlier = s < sp
        factor = jnp.where(earlier, jnp.exp(running), 0.0)
        running = running + jnp.where(earlier, gt[s // 2, s % 2], 0.0)
        for h in range(heads):
            sums[h] = sums[h] + factor[h : h + 1, :] * gs[s // 2, s % 2, h].astype(jnp.float32)
    for h in range(heads):
        entering[h] = sums[h].astype(jnp.bfloat16)
    for i in range(planes):
        p = plane_of(i)
        if i > 0:
            move(0, i, gs.at[z, x], to_x).wait_send()
            move(1, i, gt.at[z, x], to_x).wait_send()
        move(2, i, gs.at[p, x], to_x).wait_send()
        move(3, i, gt.at[p, x], to_x).wait_send()


def mix_kernel(part, out, from_core, held, from_y, ssem, rsem):
    sp, tp = lax.axis_index("sp"), lax.axis_index("tp")
    y, c = tp // 2, tp % 2
    to_core = {"sp": sp, "tp": y * 2 + (1 - c)}
    to_y = {"sp": sp, "tp": (1 - y) * 2 + c}

    def move(i, src, dst, device):
        return pltpu.make_async_remote_copy(
            src_ref=src, dst_ref=dst, send_sem=ssem.at[i], recv_sem=rsem.at[i],
            device_id=device, device_id_type=pl.DeviceIdType.MESH,
        )

    greet([to_core, to_y])
    far = move(0, part.at[1 - y, 1 - c], from_core.at[0], to_core)
    near = move(1, part.at[y, 1 - c], from_core.at[1], to_core)
    far.start()
    near.start()
    far.wait_recv()
    held[0] = (
        part[1 - y, c].astype(jnp.float32) + from_core[0].astype(jnp.float32)
    ).astype(jnp.bfloat16)
    across = move(2, held.at[0], from_y, to_y)
    across.start()
    near.wait_recv()
    mine = part[y, c].astype(jnp.float32) + from_core[1].astype(jnp.float32)
    across.wait_recv()
    out[...] = mine + from_y[...].astype(jnp.float32)
    far.wait_send()
    near.wait_send()
    across.wait_send()


def retention(query_rows, key_rows, value_rows, gate_rows, log_decay, head_gain):
    length, local_heads = log_decay.shape
    width = query_rows.shape[1]
    sp_count, mine = lax.axis_size("sp"), lax.axis_index("sp")
    positions = (mine * length + jnp.arange(length, dtype=jnp.int32)).astype(jnp.float32)
    angles = rotary_angles(positions, HEAD_DIM)
    cosine, sine = jnp.cos(angles), jnp.sin(angles)
    cosine = jnp.concatenate([cosine, cosine], axis=1)
    sine = jnp.concatenate([-sine, sine], axis=1)
    cumulative = jnp.cumsum(log_decay, axis=0)
    rows_spec = pl.BlockSpec((length, HEAD_DIM), lambda h: (0, h))
    table_spec = pl.BlockSpec((length, HEAD_DIM), lambda h: (0, 0))
    retained, qdec, state = pl.pallas_call(
        retention_kernel,
        grid=(local_heads,),
        out_shape=(
            jax.ShapeDtypeStruct((length, width), jnp.float32),
            jax.ShapeDtypeStruct((length, width), jnp.bfloat16),
            jax.ShapeDtypeStruct((local_heads, HEAD_DIM + 8, HEAD_DIM), jnp.float32),
        ),
        in_specs=[
            rows_spec,
            rows_spec,
            rows_spec,
            table_spec,
            table_spec,
            pl.BlockSpec((length, local_heads), lambda h: (0, 0)),
            pl.BlockSpec((1, 1, length), lambda h: (h, 0, 0)),
        ],
        out_specs=(
            rows_spec,
            rows_spec,
            pl.BlockSpec((1, HEAD_DIM + 8, HEAD_DIM), lambda h: (h, 0, 0)),
        ),
    )(query_rows, key_rows, value_rows, cosine, sine, cumulative, cumulative.T[:, None, :])
    if sp_count % 2 == 0 and local_heads <= 8 and sp_count <= 16:
        totals = jnp.broadcast_to(state[:, HEAD_DIM, :1], (local_heads, HEAD_DIM))
        totals = jnp.pad(totals, ((0, 8 - local_heads), (0, 0)))
        planes = sp_count // 2
        block = (local_heads, HEAD_DIM, HEAD_DIM)
        entering = pl.pallas_call(
            functools.partial(state_kernel, planes),
            out_shape=jax.ShapeDtypeStruct(block, jnp.bfloat16),
            in_specs=[pl.BlockSpec(memory_space=pltpu.VMEM)] * 2,
            out_specs=pl.BlockSpec(memory_space=pltpu.VMEM),
            scratch_shapes=[
                pltpu.VMEM((planes, 2) + block, jnp.bfloat16),
                pltpu.VMEM((planes, 2, 8, HEAD_DIM), jnp.float32),
                pltpu.SemaphoreType.DMA((4, planes)),
                pltpu.SemaphoreType.DMA((4, planes)),
                pltpu.SemaphoreType.DMA((2,)),
            ],
            compiler_params=pltpu.CompilerParams(collective_id=1, has_side_effects=True),
        )(state[:, :HEAD_DIM, :].astype(jnp.bfloat16), totals)
    else:
        pieces = lax.all_gather(state, "sp")
        totals = pieces[:, :, HEAD_DIM, 0]
        index = jnp.arange(sp_count, dtype=jnp.int32)
        between = (index[None, :] > index[:, None]) & (index[None, :] < mine)
        gap = jnp.sum(jnp.where(between[:, :, None], totals[None], 0.0), axis=1)
        factor = jnp.where((index < mine)[:, None], jnp.exp(gap), 0.0)
        entering = jnp.sum(factor[:, :, None, None] * pieces[:, :, :HEAD_DIM, :], axis=0)
    return pl.pallas_call(
        norm_kernel,
        grid=(local_heads,),
        out_shape=jax.ShapeDtypeStruct((length, width), jnp.bfloat16),
        in_specs=[
            rows_spec,
            rows_spec,
            pl.BlockSpec((1, HEAD_DIM, HEAD_DIM), lambda h: (h, 0, 0)),
            pl.BlockSpec((1, HEAD_DIM), lambda h: (0, h)),
            rows_spec,
        ],
        out_specs=rows_spec,
    )(retained, qdec, entering, head_gain[None, :], gate_rows)


Z_A, Z_B, X_A2, Y_B2, Y_A3, Y_A4, X_B3, X_B4, C_A, C_B, C_P, Y_A, X_B, X_A, Y_B, RZ_A, RZ_B = range(17)


def experts_kernel(
    planes, x0, x1, upd, wg, wu, wd, out,
    g0, g1, pm, pc, pr, a0, a1, r10, r11, b0, b1, r20, r21, d0, d1, z0, z1,
    ssem, rsem, lsem,
):
    sp, tp = lax.axis_index("sp"), lax.axis_index("tp")
    sp_count = 2 * planes
    z, x = sp // 2, sp % 2
    y, c = tp // 2, tp % 2
    half = x1.shape[1]
    rows = x1.shape[0]
    f32, bf16 = jnp.float32, jnp.bfloat16
    to_core = {"sp": sp, "tp": y * 2 + (1 - c)}
    to_y = {"sp": sp, "tp": (1 - y) * 2 + c}
    to_x = {"sp": z * 2 + (1 - x), "tp": tp}

    def plane_of(i):
        return (z + planes - i) % planes

    def to_z(i):
        return {"sp": plane_of(i) * 2 + x, "tp": tp}

    def from_z(i):
        return {"sp": ((z + i) % planes) * 2 + x, "tp": tp}

    def move(kind, i, src, dst, device):
        return pltpu.make_async_remote_copy(
            src_ref=src, dst_ref=dst, send_sem=ssem.at[kind, i], recv_sem=rsem.at[kind, i],
            device_id=device, device_id_type=pl.DeviceIdType.MESH,
        )

    def send(kind, i, src, dst, device):
        move(kind, i, src, dst, device).start()

    def arrived(kind, i, dst):
        move(kind, i, dst, dst, to_core).wait_recv()

    def left(kind, i, src):
        move(kind, i, src, src, to_core).wait_send()

    barrier = pltpu.get_barrier_semaphore()
    for device in [to_core, to_y, to_x] + [to_z(i) for i in range(1, planes)]:
        pl.semaphore_signal(barrier, inc=1, device_id=device, device_id_type=pl.DeviceIdType.MESH)
    pl.semaphore_wait(barrier, 2 + planes)

    here = x * 2 + y
    other_x = (1 - x) * 2 + y
    other_y = x * 2 + (1 - y)
    other_xy = (1 - x) * 2 + (1 - y)
    own0 = pltpu.make_async_copy(x0, g0.at[c, z, here], lsem.at[0])
    own1 = pltpu.make_async_copy(x1, g1.at[c, z, here], lsem.at[1])
    own0.start()
    own1.start()
    own0.wait()
    own1.wait()
    for i in range(1, planes):
        send(Z_A, i, g0.at[c, z, here], g0.at[c, z, here], from_z(i))
        send(Z_B, i, g1.at[c, z, here], g1.at[c, z, here], from_z(i))

    def compute(i, core):
        p = plane_of(i)
        left_rows = g0[core, p].reshape(4 * rows, half + 128)
        right_rows = g1[core, p].reshape(4 * rows, half)
        tail = left_rows[:, half:].astype(f32)
        left_rows = left_rows[:, :half]
        lane = lax.broadcasted_iota(jnp.int32, tail.shape, 1)
        weight = jnp.sum(
            jnp.where((lane == sp) | (lane == sp + sp_count), tail, 0.0), axis=1, keepdims=True
        )

        def product(w):
            return jnp.dot(left_rows, w[:half, :], preferred_element_type=f32) + jnp.dot(
                right_rows, w[half:, :], preferred_element_type=f32
            )

        gate = jnp.minimum(product(wg), clamp_limit)
        up = jnp.clip(product(wu), -clamp_limit, clamp_limit)
        act = ((up + 1.0) * (gate / (1.0 + jnp.exp(-swish_alpha * gate)))).astype(bf16)
        return (jnp.dot(act, wd[...], preferred_element_type=f32) * weight).astype(bf16)

    def step(i, carry):
        @pl.when((i >= 1) & (i < planes + 1))
        def _():
            j = i - 1
            p = plane_of(j)
            arrived(Y_A3, j, g0.at[c, p, other_y])
            arrived(Y_A4, j, g0.at[c, p, other_xy])
            arrived(X_B3, j, g1.at[c, p, other_x])
            arrived(X_B4, j, g1.at[c, p, other_xy])
            send(C_A, j, g0.at[c, p], g0.at[c, p], to_core)
            send(C_B, j, g1.at[c, p], g1.at[c, p], to_core)

        @pl.when(i < planes)
        def _():
            p = plane_of(i)

            @pl.when(i > 0)
            def _():
                arrived(Z_A, i, g0.at[c, p, here])
                arrived(Z_B, i, g1.at[c, p, here])

            send(X_A2, i, g0.at[c, p, here], g0.at[c, p, here], to_x)
            send(Y_B2, i, g1.at[c, p, here], g1.at[c, p, here], to_y)
            send(Y_A3, i, g0.at[c, p, here], g0.at[c, p, here], to_y)
            send(X_B3, i, g1.at[c, p, here], g1.at[c, p, here], to_x)
            arrived(X_A2, i, g0.at[c, p, other_x])
            send(Y_A4, i, g0.at[c, p, other_x], g0.at[c, p, other_x], to_y)
            arrived(Y_B2, i, g1.at[c, p, other_y])
            send(X_B4, i, g1.at[c, p, other_y], g1.at[c, p, other_y], to_x)

        @pl.when((i >= 2) & (i < planes + 2))
        def _():
            j = i - 2
            arrived(C_P, j, pr.at[j])
            for q in range(4):
                part = pl.ds(q * rows, rows)
                total = (pm[j, part, :].astype(f32) + pr[j, part, :].astype(f32)).astype(bf16)
                a0[j, q % 2, q // 2] = total[:, :half]
                a1[j, q // 2, q % 2] = total[:, half:]
            send(Y_A, j, a0.at[j, 1 - y], r10.at[j], to_y)
            send(X_B, j, a1.at[j, 1 - x], r11.at[j], to_x)

        @pl.when((i >= 3) & (i < planes + 3))
        def _():
            j = i - 3
            arrived(Y_A, j, r10.at[j])
            b0[j] = (a0[j, y].astype(f32) + r10[j].astype(f32)).astype(bf16)
            send(X_A, j, b0.at[j, 1 - x], r20.at[j], to_x)
            arrived(X_B, j, r11.at[j])
            b1[j] = (a1[j, x].astype(f32) + r11[j].astype(f32)).astype(bf16)
            send(Y_B, j, b1.at[j, 1 - y], r21.at[j], to_y)

        @pl.when((i >= 4) & (i < planes + 4))
        def _():
            j = i - 4
            arrived(X_A, j, r20.at[j])
            d0[j] = (b0[j, x].astype(f32) + r20[j].astype(f32)).astype(bf16)
            arrived(Y_B, j, r21.at[j])
            d1[j] = (b1[j, y].astype(f32) + r21[j].astype(f32)).astype(bf16)

            @pl.when(j > 0)
            def _():
                send(RZ_A, j, d0.at[j], z0.at[j], to_z(j))
                send(RZ_B, j, d1.at[j], z1.at[j], to_z(j))

        @pl.when((i >= 1) & (i < planes + 1))
        def _():
            j = i - 1
            p = plane_of(j)
            arrived(C_A, j, g0.at[1 - c, p])
            arrived(C_B, j, g1.at[1 - c, p])

            def tile(turn, carry):
                @pl.when(turn == 0)
                def _():
                    pc[j] = compute(j, 1 - c)
                    send(C_P, j, pc.at[j], pr.at[j], to_core)

                @pl.when(turn == 1)
                def _():
                    pm[j] = compute(j, c)

                return carry

            lax.fori_loop(0, 2, tile, 0)

        return carry

    lax.fori_loop(0, planes + 4, step, 0)
    low, high = upd[:, :half], upd[:, half:]
    low = low + d0[0].astype(f32)
    high = high + d1[0].astype(f32)
    for i in range(1, planes):
        arrived(RZ_A, i, z0.at[i])
        low = low + z0[i].astype(f32)
        arrived(RZ_B, i, z1.at[i])
        high = high + z1[i].astype(f32)
    out[:, :half] = low.astype(bf16)
    out[:, half:] = high.astype(bf16)

    def drain(i, carry):
        p = plane_of(i)

        @pl.when(i > 0)
        def _():
            left(Z_A, i, g0.at[c, z, here])
            left(Z_B, i, g1.at[c, z, here])
            left(RZ_A, i, d0.at[i])
            left(RZ_B, i, d1.at[i])

        left(X_A2, i, g0.at[c, p, here])
        left(Y_B2, i, g1.at[c, p, here])
        left(Y_A3, i, g0.at[c, p, here])
        left(X_B3, i, g1.at[c, p, here])
        left(Y_A4, i, g0.at[c, p, other_x])
        left(X_B4, i, g1.at[c, p, other_y])
        left(C_A, i, g0.at[c, p])
        left(C_B, i, g1.at[c, p])
        left(C_P, i, pc.at[i])
        left(Y_A, i, a0.at[i, 1 - y])
        left(X_B, i, a1.at[i, 1 - x])
        left(X_A, i, b0.at[i, 1 - x])
        left(Y_B, i, b1.at[i, 1 - y])
        return carry

    lax.fori_loop(0, planes, drain, 0)


def dense_experts(updated, ffn_in, own_routes, route_weights, gate_part, up_part, down_part):
    sp_count, mine = lax.axis_size("sp"), lax.axis_index("sp")
    width = ffn_in.shape[1]
    chosen = own_routes[:, :, None] == jnp.arange(sp_count, dtype=jnp.int32)[None, None, :]
    shares = jnp.sum(jnp.where(chosen, route_weights[:, :, None], 0.0), axis=1)
    coarse = shares.astype(jnp.bfloat16)
    fine = (shares - coarse.astype(jnp.float32)).astype(jnp.bfloat16)
    spare = jnp.zeros((ffn_in.shape[0], 128 - 2 * sp_count), jnp.bfloat16)
    half = width // 2
    first = jnp.concatenate([ffn_in[:, :half], coarse, fine, spare], axis=1)
    second = ffn_in[:, half:]
    rows = ffn_in.shape[0]
    planes = sp_count // 2
    bf16 = jnp.bfloat16
    whole = pl.BlockSpec(memory_space=pltpu.VMEM)
    return pl.pallas_call(
        functools.partial(experts_kernel, planes),
        out_shape=jax.ShapeDtypeStruct((rows, width), bf16),
        in_specs=[whole] * 6,
        out_specs=whole,
        scratch_shapes=[
            pltpu.VMEM((2, planes, 4, rows, half + 128), bf16),
            pltpu.VMEM((2, planes, 4, rows, half), bf16),
            pltpu.VMEM((planes, 4 * rows, width), bf16),
            pltpu.VMEM((planes, 4 * rows, width), bf16),
            pltpu.VMEM((planes, 4 * rows, width), bf16),
            pltpu.VMEM((planes, 2, 2, rows, half), bf16),
            pltpu.VMEM((planes, 2, 2, rows, half), bf16),
            pltpu.VMEM((planes, 2, rows, half), bf16),
            pltpu.VMEM((planes, 2, rows, half), bf16),
            pltpu.VMEM((planes, 2, rows, half), bf16),
            pltpu.VMEM((planes, 2, rows, half), bf16),
            pltpu.VMEM((planes, rows, half), bf16),
            pltpu.VMEM((planes, rows, half), bf16),
            pltpu.VMEM((planes, rows, half), bf16),
            pltpu.VMEM((planes, rows, half), bf16),
            pltpu.VMEM((planes, rows, half), bf16),
            pltpu.VMEM((planes, rows, half), bf16),
            pltpu.SemaphoreType.DMA((17, planes)),
            pltpu.SemaphoreType.DMA((17, planes)),
            pltpu.SemaphoreType.DMA((2,)),
        ],
        compiler_params=pltpu.CompilerParams(
            collective_id=0, has_side_effects=True, vmem_limit_bytes=63 * 1024 * 1024
        ),
    )(first, second, updated, gate_part, up_part, down_part)


def body(
    query_rows,
    key_rows,
    value_rows,
    gate_rows,
    log_decay,
    head_gain,
    out_weight,
    residual,
    ffn_gain,
    gate_weight,
    up_weight,
    down_weight,
    routes,
    route_weights,
):
    tok_count = query_rows.shape[0]
    local_heads = log_decay.shape[1]
    sp_count = lax.axis_size("sp")
    tp_count = lax.axis_size("tp")
    model_width = residual.shape[1]
    rows_own = tok_count // tp_count
    capacity = max(2, 3 * rows_own * TOPK // (2 * sp_count))
    hidden = retention(query_rows, key_rows, value_rows, gate_rows, log_decay, head_gain)
    mixed = jnp.dot(hidden, out_weight, preferred_element_type=jnp.float32).astype(jnp.bfloat16)
    if tp_count == 4 and sp_count <= 16:
        mixed_sum = pl.pallas_call(
            mix_kernel,
            out_shape=jax.ShapeDtypeStruct((rows_own, model_width), jnp.float32),
            in_specs=[pl.BlockSpec(memory_space=pltpu.VMEM)],
            out_specs=pl.BlockSpec(memory_space=pltpu.VMEM),
            scratch_shapes=[
                pltpu.VMEM((2, rows_own, model_width), jnp.bfloat16),
                pltpu.VMEM((2, rows_own, model_width), jnp.bfloat16),
                pltpu.VMEM((rows_own, model_width), jnp.bfloat16),
                pltpu.SemaphoreType.DMA((3,)),
                pltpu.SemaphoreType.DMA((3,)),
            ],
            compiler_params=pltpu.CompilerParams(collective_id=2, has_side_effects=True),
        )(mixed.reshape(2, 2, rows_own, model_width))
    else:
        mixed_sum = lax.psum_scatter(mixed, "tp", scatter_dimension=0, tiled=True).astype(
            jnp.float32
        )
    updated = residual.astype(jnp.float32) + mixed_sum
    ffn_in = square_norm(updated, ffn_gain)
    tp_index = lax.axis_index("tp")
    own_routes = lax.dynamic_slice_in_dim(routes, tp_index * rows_own, rows_own, 0)
    if rows_own < 2 * capacity and 2 * sp_count <= 128 and sp_count % 2 == 0 and tp_count == 4:
        return dense_experts(
            updated, ffn_in, own_routes, route_weights, gate_weight[0], up_weight[0], down_weight[0]
        )
    own_experts, own_ranks = slot_ranks(own_routes, sp_count)
    home_slot = own_experts * capacity + own_ranks
    gate_part = gate_weight[0]
    up_part = up_weight[0]
    down_part = down_weight[0]
    empty_row = jnp.zeros((1, model_width), jnp.bfloat16)
    source_row = (
        jnp.full((sp_count * capacity,), rows_own, jnp.int32)
        .at[home_slot]
        .set(jnp.arange(rows_own * TOPK, dtype=jnp.int32) // TOPK)
    )
    padded = jnp.concatenate([ffn_in, empty_row], axis=0)
    outgoing = padded[source_row].reshape(sp_count, capacity, model_width)
    arrived = lax.all_to_all(outgoing, "sp", split_axis=0, concat_axis=0, tiled=True)
    fanned = lax.all_gather(arrived[None], "tp", axis=0, tiled=True)
    activity = expert_rows(fanned.reshape(-1, model_width), gate_part, up_part)
    partial_out = jnp.dot(activity, down_part, preferred_element_type=jnp.float32).reshape(
        tp_count, sp_count, capacity, model_width
    )
    summed = (
        lax.psum_scatter(partial_out.astype(jnp.bfloat16), "tp", scatter_dimension=0, tiled=True)
        .astype(jnp.float32)
        .reshape(sp_count, capacity, model_width)
    )
    returned = lax.all_to_all(
        summed.astype(jnp.bfloat16), "sp", split_axis=0, concat_axis=0, tiled=True
    )
    picked = returned.reshape(sp_count * capacity, model_width)[home_slot].reshape(
        rows_own, TOPK, model_width
    )
    expert_sum = jnp.sum(route_weights[:, :, None] * picked.astype(jnp.float32), axis=1)
    return (updated + expert_sum).astype(jnp.bfloat16)


def solution(mesh):
    return jax.shard_map(
        body,
        mesh=mesh,
        in_specs=(
            P("sp", "tp"),
            P("sp", "tp"),
            P("sp", "tp"),
            P("sp", "tp"),
            P("sp", "tp"),
            P("tp"),
            P("tp", None),
            P(("sp", "tp"), None),
            P(),
            P("sp", None, "tp"),
            P("sp", None, "tp"),
            P("sp", "tp", None),
            P("sp", None),
            P(("sp", "tp"), None),
        ),
        out_specs=P(("sp", "tp"), None),
        check_vma=False,
    )
```

profile of v0, /device:TPU:0, one launch (start us, length us, event | category | flops | bytes accessed | tf_op | source)
XLA Modules:
  0.0 166.0 jit_solution(16813410180597801080)
XLA Ops:
  0.0 0.5 fusion
  0.6 0.8 pad_maximum_fusion
  1.4 0.7 reshape.49
  2.1 1.2 reduce-window.6
  3.4 0.1 copy.30
  3.6 0.1 copy.31
  3.7 0.8 copy.32
  4.5 4.3 %shard_map.136 = (f32[256,512]{1,0:T(8,128)}, bf16[256,512]{1,0:T(8,128)(2,1)}, f32[4,136,128]{2,1,0:T(8,128)}) custom-call(bf16[256,512]{1,0:T(8,128)(2,1)} %q_ref.1, bf16[256,512]{1,0:T(8,128)(2,1)} %k_ref.1, bf16[256,512]{1,0:T(8,128)(2,1)} %v_ref.1, f32[256,128]{1,0:T(8,128)} %get-tuple-element.18.cos_ref, f32[256,128]{1,0:T(8,128)} %get-tuple-element.19.sin_ref, ...), custom_call_target="tpu_custom_call" | custom-call | tf_op jit(solution)/shard_map/pallas_call | solution.py:212
  8.9 1.6 slice.31.state
  10.5 0.8 slice_reduce_fusion
  11.3 0.6 pad.7.totals
  12.0 25.1 %shard_map.137.enter_ref = bf16[4,128,128]{2,1,0:T(8,128)(2,1)} custom-call(bf16[4,128,128]{2,1,0:T(8,128)(2,1)} %slice.31.state, f32[8,128]{1,0:T(8,128)} %pad.7.totals), custom_call_target="tpu_custom_call" | custom-call | tf_op jit(solution)/shard_map/pallas_call | solution.py:240
  37.1 3.9 %shard_map.138 = bf16[256,512]{1,0:T(8,128)(2,1)} custom-call(f32[256,512]{1,0:T(8,128)} %get-tuple-element.8.ret_ref, bf16[256,512]{1,0:T(8,128)(2,1)} %get-tuple-element.9.qdec_ref, bf16[4,128,128]{2,1,0:T(8,128)(2,1)} %shard_map.137.enter_ref, f32[1,512]{1,0:T(1,128)} %bitcast.21, bf16[256,512]{1,0:T(8,128)(2,1)} %gate_ref.1), custom_call_target="tpu_custom_call" | custom-call | tf_op jit(solution)/shard_map/pallas_call | solution.py:262
  41.1 2.7 %convolution_convert_fusion = bf16[256,2048]{1,0:T(8,128)(2,1)} fusion(bf16[256,512]{1,0:T(8,128)(2,1)} %shard_map.138, bf16[512,2048]{1,0:T(8,128)(2,1)S(1)} %copy-done.2), kind=kOutput, calls=%fused_computation | convolution fusion | flops 537395200 | bytes 3407872 | tf_op jit(solution)/shard_map/dot_general | solution.py:560
  43.8 12.3 %shard_map.139 = f32[64,2048]{1,0:T(8,128)} custom-call(bf16[2,2,64,2048]{3,2,1,0:T(8,128)(2,1)} %bitcast.13), custom_call_target="tpu_custom_call" | custom-call | tf_op jit(solution)/shard_map/pallas_call | solution.py:562
  56.1 1.2 multiply_reduce_fusion
  57.4 0.1 multiply_convert_fusion
  57.5 0.7 fusion.1
  58.3 0.1 copy.34
  58.4 0.1 copy.33
  58.4 0.1 copy.35
  58.6 0.8 concatenate.11.x0
  59.3 105.0 %shard_map.140 = bf16[64,2048]{1,0:T(8,128)(2,1)} custom-call(bf16[64,1152]{1,0:T(8,128)(2,1)} %concatenate.11.x0, bf16[64,1024]{1,0:T(8,128)(2,1)} %get-tuple-element.13.x1, f32[64,2048]{1,0:T(8,128)} %copy-done.1, bf16[2048,512]{1,0:T(8,128)(2,1)} %bitcast.14, bf16[2048,512]{1,0:T(8,128)(2,1)} %bitcast.15, bf16[512,2048]{1,0:T(8,128)(2,1)} %bitcast.16), custom_call_target="tpu_custom_call" | custom-call | tf_op jit(solution)/shard_map/pallas_call | solution.py:503
  164.3 1.7 %copy.37 = bf16[64,2048]{1,0:T(8,128)(2,1)} copy(bf16[64,2048]{1,0:T(8,128)(2,1)} %shard_map.140) | data formatting | bytes 524288
  (27 shorter events, 0.3 us)
Async XLA Ops:
  0.0 58.2 %copy-start = (s32[256,4]{0,1:T(4,128)S(1)}, s32[256,4]{0,1:T(4,128)}, u32[]{:S(2)}) copy-start(s32[256,4]{0,1:T(4,128)} %param.26) | copy-start | bytes 12292
  0.6 40.5 %copy-start.2 = (bf16[512,2048]{1,0:T(8,128)(2,1)S(1)}, bf16[512,2048]{1,0:T(8,128)(2,1)}, u32[]{:S(2)}) copy-start(bf16[512,2048]{1,0:T(8,128)(2,1)} %param.20) | copy-start | bytes 6291460
  3.7 0.8 copy-start.4
  41.1 15.0 %copy-start.3 = (bf16[64,2048]{1,0:T(8,128)(2,1)S(1)}, bf16[64,2048]{1,0:T(8,128)(2,1)}, u32[]{:S(2)}) copy-start(bf16[64,2048]{1,0:T(8,128)(2,1)} %param.21) | copy-start | bytes 786436
  43.8 13.5 %copy-start.5 = (f32[2048]{0:T(1024)S(1)}, f32[2048]{0:T(1024)}, u32[]{:S(2)}) copy-start(f32[2048]{0:T(1024)} %param.22) | copy-start | bytes 24580
  43.8 14.4 %copy-start.6 = (f32[64,4]{0,1:T(4,128)S(1)}, f32[64,4]{0,1:T(4,128)}, u32[]{:S(2)}) copy-start(f32[64,4]{0,1:T(4,128)} %param.27) | copy-start | bytes 3076
  57.3 2.0 %copy-start.1 = (f32[64,2048]{1,0:T(8,128)}, f32[64,2048]{1,0:T(8,128)S(1)}, u32[]{:S(2)}) copy-start(f32[64,2048]{1,0:T(8,128)S(1)} %get-tuple-element.12.upd) | copy-start | bytes 1572868
where the time goes:
time: 166 us
  Pallas kernels  151 us (91%)
  local copies, waits for them, and re-layouts  8.38 us (5%)
  other arithmetic  4.08 us (2%)
  matrix products  2.73 us (2%)
    pallas_call x1, Pallas kernels, dense_experts(): pl.pallas_call(functools.partial(experts_kernel, planes), out_shape=jax.S...  105 us
    pallas_call x1, Pallas kernels, retention(): pl.pallas_call(functools.partial(state_kernel, planes), out_shape=jax.Sha...  25.1 us
    pallas_call x1, Pallas kernels, body(): pl.pallas_call(mix_kernel, out_shape=jax.ShapeDtypeStruct((rows_own, mode...  12.3 us
    pallas_call x1, Pallas kernels, retention(): pl.pallas_call(retention_kernel, grid=(local_heads,), out_shape=(jax.Shap...  4.35 us
    pallas_call x1, Pallas kernels, retention(): pl.pallas_call(norm_kernel, grid=(local_heads,), out_shape=jax.ShapeDtype...  3.95 us

commit v1 on v0

--- a/solution.py
+++ b/solution.py
@@ -278,211 +278,223 @@
 
 
 def experts_kernel(
-    planes, x0, x1, upd, wg, wu, wd, out,
-    g0, g1, pm, pc, pr, a0, a1, r10, r11, b0, b1, r20, r21, d0, d1, z0, z1,
-    ssem, rsem, lsem,
+    planes, x0, x1, upd, wg_hbm, wu_hbm, wd_hbm, out,
+    wg, wu, wd, g0, g1, pm, pr, a0, a1, r10, r11, b0, b1, r20, r21, d0, d1, z0, z1,
+    ssem, rsem, lsem, wsem,
 ):
     sp, tp = lax.axis_index("sp"), lax.axis_index("tp")
     sp_count = 2 * planes
     z, x = sp // 2, sp % 2
     y, c = tp // 2, tp % 2
     half = x1.shape[1]
-    rows = x1.shape[0]
+    rows = x1.shape[0] // 2
+    items = 2 * planes
     f32, bf16 = jnp.float32, jnp.bfloat16
     to_core = {"sp": sp, "tp": y * 2 + (1 - c)}
     to_y = {"sp": sp, "tp": (1 - y) * 2 + c}
     to_x = {"sp": z * 2 + (1 - x), "tp": tp}
 
-    def plane_of(i):
-        return (z + planes - i) % planes
+    def item_of(i, r):
+        return (items - 1) * r if i == 0 else 2 * i - 1 + r
+
+    def turn_of(n):
+        return ((n + 1) // 2) % planes
 
     def to_z(i):
-        return {"sp": plane_of(i) * 2 + x, "tp": tp}
+        return {"sp": ((z + planes - i) % planes) * 2 + x, "tp": tp}
 
     def from_z(i):
         return {"sp": ((z + i) % planes) * 2 + x, "tp": tp}
 
-    def move(kind, i, src, dst, device):
+    def move(kind, n, src, dst, device):
         return pltpu.make_async_remote_copy(
-            src_ref=src, dst_ref=dst, send_sem=ssem.at[kind, i], recv_sem=rsem.at[kind, i],
+            src_ref=src, dst_ref=dst, send_sem=ssem.at[kind, n], recv_sem=rsem.at[kind, n],
             device_id=device, device_id_type=pl.DeviceIdType.MESH,
         )
 
-    def send(kind, i, src, dst, device):
-        move(kind, i, src, dst, device).start()
-
-    def arrived(kind, i, dst):
-        move(kind, i, dst, dst, to_core).wait_recv()
-
-    def left(kind, i, src):
-        move(kind, i, src, src, to_core).wait_send()
+    def send(kind, n, src, dst, device):
+        move(kind, n, src, dst, device).start()
+
+    def arrived(kind, n, dst):
+        move(kind, n, dst, dst, to_core).wait_recv()
+
+    def left(kind, n, src):
+        move(kind, n, src, src, to_core).wait_send()
 
     barrier = pltpu.get_barrier_semaphore()
     for device in [to_core, to_y, to_x] + [to_z(i) for i in range(1, planes)]:
         pl.semaphore_signal(barrier, inc=1, device_id=device, device_id_type=pl.DeviceIdType.MESH)
-    pl.semaphore_wait(barrier, 2 + planes)
 
     here = x * 2 + y
     other_x = (1 - x) * 2 + y
     other_y = x * 2 + (1 - y)
     other_xy = (1 - x) * 2 + (1 - y)
-    own0 = pltpu.make_async_copy(x0, g0.at[c, z, here], lsem.at[0])
-    own1 = pltpu.make_async_copy(x1, g1.at[c, z, here], lsem.at[1])
-    own0.start()
-    own1.start()
-    own0.wait()
-    own1.wait()
+    own = []
+    for r in range(2):
+        n, part = item_of(0, r), pl.ds(r * rows, rows)
+        own.append(pltpu.make_async_copy(x0.at[part], g0.at[c, n, here], lsem.at[2 * r]))
+        own.append(pltpu.make_async_copy(x1.at[part], g1.at[c, n, here], lsem.at[2 * r + 1]))
+    for copy in own:
+        copy.start()
+    weights = [
+        pltpu.make_async_copy(wg_hbm, wg, wsem.at[0]),
+        pltpu.make_async_copy(wu_hbm, wu, wsem.at[1]),
+        pltpu.make_async_copy(wd_hbm, wd, wsem.at[2]),
+    ]
+    for copy in weights:
+        copy.start()
+    for copy in own:
+        copy.wait()
+    pl.semaphore_wait(barrier, 2 + planes)
+
+    def spread(n):
+        send(X_A2, n, g0.at[c, n, here], g0.at[c, n, here], to_x)
+        send(Y_B2, n, g1.at[c, n, here], g1.at[c, n, here], to_y)
+        send(Y_A3, n, g0.at[c, n, here], g0.at[c, n, here], to_y)
+        send(X_B3, n, g1.at[c, n, here], g1.at[c, n, here], to_x)
+
+    spread(0)
     for i in range(1, planes):
-        send(Z_A, i, g0.at[c, z, here], g0.at[c, z, here], from_z(i))
-        send(Z_B, i, g1.at[c, z, here], g1.at[c, z, here], from_z(i))
-
-    def compute(i, core):
-        p = plane_of(i)
-        left_rows = g0[core, p].reshape(4 * rows, half + 128)
-        right_rows = g1[core, p].reshape(4 * rows, half)
-        tail = left_rows[:, half:].astype(f32)
-        left_rows = left_rows[:, :half]
-        lane = lax.broadcasted_iota(jnp.int32, tail.shape, 1)
-        weight = jnp.sum(
-            jnp.where((lane == sp) | (lane == sp + sp_count), tail, 0.0), axis=1, keepdims=True
-        )
-
-        def product(w):
-            return jnp.dot(left_rows, w[:half, :], preferred_element_type=f32) + jnp.dot(
-                right_rows, w[half:, :], preferred_element_type=f32
+        for r in range(2):
+            n, m = item_of(i, r), item_of(0, r)
+            send(Z_A, n, g0.at[c, m, here], g0.at[c, n, here], from_z(i))
+            send(Z_B, n, g1.at[c, m, here], g1.at[c, n, here], from_z(i))
+
+    def tick(t, carry):
+        @pl.when(t < items)
+        def _():
+            arrived(X_A2, t, g0.at[c, t, other_x])
+            send(Y_A4, t, g0.at[c, t, other_x], g0.at[c, t, other_x], to_y)
+            arrived(Y_B2, t, g1.at[c, t, other_y])
+            send(X_B4, t, g1.at[c, t, other_y], g1.at[c, t, other_y], to_x)
+
+        @pl.when(t + 1 < items)
+        def _():
+            n = t + 1
+
+            @pl.when(n < items - 1)
+            def _():
+                arrived(Z_A, n, g0.at[c, n, here])
+                arrived(Z_B, n, g1.at[c, n, here])
+
+            spread(n)
+
+        @pl.when(t == 2)
+        def _():
+            for copy in weights:
+                copy.wait()
+
+        @pl.when((t >= 2) & (t < items + 2))
+        def _():
+            n = t - 2
+            arrived(C_A, n, g0.at[1 - c, n])
+            arrived(C_B, n, g1.at[1 - c, n])
+            lead = g0[:, n].reshape(8 * rows, half + 128)
+            tail = lead[:, half:].astype(f32)
+            lead = lead[:, :half]
+            rest = g1[:, n].reshape(8 * rows, half)
+            lane = lax.broadcasted_iota(jnp.int32, tail.shape, 1)
+            weight = jnp.sum(
+                jnp.where((lane == sp) | (lane == sp + sp_count), tail, 0.0), axis=1, keepdims=True
             )
 
-        gate = jnp.minimum(product(wg), clamp_limit)
-        up = jnp.clip(product(wu), -clamp_limit, clamp_limit)
-        act = ((up + 1.0) * (gate / (1.0 + jnp.exp(-swish_alpha * gate)))).astype(bf16)
-        return (jnp.dot(act, wd[...], preferred_element_type=f32) * weight).astype(bf16)
-
-    def step(i, carry):
-        @pl.when((i >= 1) & (i < planes + 1))
-        def _():
-            j = i - 1
-            p = plane_of(j)
-            arrived(Y_A3, j, g0.at[c, p, other_y])
-            arrived(Y_A4, j, g0.at[c, p, other_xy])
-            arrived(X_B3, j, g1.at[c, p, other_x])
-            arrived(X_B4, j, g1.at[c, p, other_xy])
-            send(C_A, j, g0.at[c, p], g0.at[c, p], to_core)
-            send(C_B, j, g1.at[c, p], g1.at[c, p], to_core)
-
-        @pl.when(i < planes)
-        def _():
-            p = plane_of(i)
-
-            @pl.when(i > 0)
-            def _():
-                arrived(Z_A, i, g0.at[c, p, here])
-                arrived(Z_B, i, g1.at[c, p, here])
-
-            send(X_A2, i, g0.at[c, p, here], g0.at[c, p, here], to_x)
-            send(Y_B2, i, g1.at[c, p, here], g1.at[c, p, here], to_y)
-            send(Y_A3, i, g0.at[c, p, here], g0.at[c, p, here], to_y)
-            send(X_B3, i, g1.at[c, p, here], g1.at[c, p, here], to_x)
-            arrived(X_A2, i, g0.at[c, p, other_x])
-            send(Y_A4, i, g0.at[c, p, other_x], g0.at[c, p, other_x], to_y)
-            arrived(Y_B2, i, g1.at[c, p, other_y])
-            send(X_B4, i, g1.at[c, p, other_y], g1.at[c, p, other_y], to_x)
-
-        @pl.when((i >= 2) & (i < planes + 2))
-        def _():
-            j = i - 2
-            arrived(C_P, j, pr.at[j])
+            def product(w):
+                return jnp.dot(lead, w[:half, :], preferred_element_type=f32) + jnp.dot(
+                    rest, w[half:, :], preferred_element_type=f32
+                )
+
+            gate = jnp.minimum(product(wg), clamp_limit)
+            up = jnp.clip(product(wu), -clamp_limit, clamp_limit)
+            act = ((up + 1.0) * (gate / (1.0 + jnp.exp(-swish_alpha * gate)))).astype(bf16)
+            made = (jnp.dot(act, wd[...], preferred_element_type=f32) * weight).astype(bf16)
+            pm[n] = made.reshape(2, 4 * rows, 2 * half)
+            send(C_P, n, pm.at[n, 1 - c], pr.at[n], to_core)
+
+        @pl.when((t >= 1) & (t < items + 1))
+        def _():
+            n = t - 1
+            arrived(Y_A3, n, g0.at[c, n, other_y])
+            arrived(Y_A4, n, g0.at[c, n, other_xy])
+            arrived(X_B3, n, g1.at[c, n, other_x])
+            arrived(X_B4, n, g1.at[c, n, other_xy])
+            send(C_A, n, g0.at[c, n], g0.at[c, n], to_core)
+            send(C_B, n, g1.at[c, n], g1.at[c, n], to_core)
+
+        @pl.when((t >= 3) & (t < items + 3))
+        def _():
+            n = t - 3
+            arrived(C_P, n, pr.at[n])
             for q in range(4):
                 part = pl.ds(q * rows, rows)
-                total = (pm[j, part, :].astype(f32) + pr[j, part, :].astype(f32)).astype(bf16)
-                a0[j, q % 2, q // 2] = total[:, :half]
-                a1[j, q // 2, q % 2] = total[:, half:]
-            send(Y_A, j, a0.at[j, 1 - y], r10.at[j], to_y)
-            send(X_B, j, a1.at[j, 1 - x], r11.at[j], to_x)
-
-        @pl.when((i >= 3) & (i < planes + 3))
-        def _():
-            j = i - 3
-            arrived(Y_A, j, r10.at[j])
-            b0[j] = (a0[j, y].astype(f32) + r10[j].astype(f32)).astype(bf16)
-            send(X_A, j, b0.at[j, 1 - x], r20.at[j], to_x)
-            arrived(X_B, j, r11.at[j])
-            b1[j] = (a1[j, x].astype(f32) + r11[j].astype(f32)).astype(bf16)
-            send(Y_B, j, b1.at[j, 1 - y], r21.at[j], to_y)
-
-        @pl.when((i >= 4) & (i < planes + 4))
-        def _():
-            j = i - 4
-            arrived(X_A, j, r20.at[j])
-            d0[j] = (b0[j, x].astype(f32) + r20[j].astype(f32)).astype(bf16)
-            arrived(Y_B, j, r21.at[j])
-            d1[j] = (b1[j, y].astype(f32) + r21[j].astype(f32)).astype(bf16)
-
-            @pl.when(j > 0)
+                total = (pm[n, c, part, :].astype(f32) + pr[n, part, :].astype(f32)).astype(bf16)
+                a0[n, q % 2, q // 2] = total[:, :half]
+                a1[n, q // 2, q % 2] = total[:, half:]
+            send(Y_A, n, a0.at[n, 1 - y], r10.at[n], to_y)
+            send(X_B, n, a1.at[n, 1 - x], r11.at[n], to_x)
+
+        @pl.when((t >= 4) & (t < items + 4))
+        def _():
+            n = t - 4
+            arrived(Y_A, n, r10.at[n])
+            b0[n] = (a0[n, y].astype(f32) + r10[n].astype(f32)).astype(bf16)
+            send(X_A, n, b0.at[n, 1 - x], r20.at[n], to_x)
+            arrived(X_B, n, r11.at[n])
+            b1[n] = (a1[n, x].astype(f32) + r11[n].astype(f32)).astype(bf16)
+            send(Y_B, n, b1.at[n, 1 - y], r21.at[n], to_y)
+
+        @pl.when(t >= 5)
+        def _():
+            n = t - 5
+            arrived(X_A, n, r20.at[n])
+            d0[n] = (b0[n, x].astype(f32) + r20[n].astype(f32)).astype(bf16)
+            arrived(Y_B, n, r21.at[n])
+            d1[n] = (b1[n, y].astype(f32) + r21[n].astype(f32)).astype(bf16)
+
+            @pl.when((n > 0) & (n < items - 1))
             def _():
-                send(RZ_A, j, d0.at[j], z0.at[j], to_z(j))
-                send(RZ_B, j, d1.at[j], z1.at[j], to_z(j))
-
-        @pl.when((i >= 1) & (i < planes + 1))
-        def _():
-            j = i - 1
-            p = plane_of(j)
-            arrived(C_A, j, g0.at[1 - c, p])
-            arrived(C_B, j, g1.at[1 - c, p])
-
-            def tile(turn, carry):
-                @pl.when(turn == 0)
-                def _():
-                    pc[j] = compute(j, 1 - c)
-                    send(C_P, j, pc.at[j], pr.at[j], to_core)
-
-                @pl.when(turn == 1)
-                def _():
-                    pm[j] = compute(j, c)
-
-                return carry
-
-            lax.fori_loop(0, 2, tile, 0)
+                send(RZ_A, n, d0.at[n], z0.at[n], to_z(turn_of(n)))
+                send(RZ_B, n, d1.at[n], z1.at[n], to_z(turn_of(n)))
 
         return carry
 
-    lax.fori_loop(0, planes + 4, step, 0)
-    low, high = upd[:, :half], upd[:, half:]
-    low = low + d0[0].astype(f32)
-    high = high + d1[0].astype(f32)
-    for i in range(1, planes):
-        arrived(RZ_A, i, z0.at[i])
-        low = low + z0[i].astype(f32)
-        arrived(RZ_B, i, z1.at[i])
-        high = high + z1[i].astype(f32)
-    out[:, :half] = low.astype(bf16)
-    out[:, half:] = high.astype(bf16)
-
-    def drain(i, carry):
-        p = plane_of(i)
-
-        @pl.when(i > 0)
-        def _():
-            left(Z_A, i, g0.at[c, z, here])
-            left(Z_B, i, g1.at[c, z, here])
-            left(RZ_A, i, d0.at[i])
-            left(RZ_B, i, d1.at[i])
-
-        left(X_A2, i, g0.at[c, p, here])
-        left(Y_B2, i, g1.at[c, p, here])
-        left(Y_A3, i, g0.at[c, p, here])
-        left(X_B3, i, g1.at[c, p, here])
-        left(Y_A4, i, g0.at[c, p, other_x])
-        left(X_B4, i, g1.at[c, p, other_y])
-        left(C_A, i, g0.at[c, p])
-        left(C_B, i, g1.at[c, p])
-        left(C_P, i, pc.at[i])
-        left(Y_A, i, a0.at[i, 1 - y])
-        left(X_B, i, a1.at[i, 1 - x])
-        left(X_A, i, b0.at[i, 1 - x])
-        left(Y_B, i, b1.at[i, 1 - y])
+    lax.fori_loop(0, items + 5, tick, 0)
+    for r in range(2):
+        n, part = item_of(0, r), pl.ds(r * rows, rows)
+        low = upd[part, :half] + d0[n].astype(f32)
+        high = upd[part, half:] + d1[n].astype(f32)
+        for i in range(1, planes):
+            n = item_of(i, r)
+            arrived(RZ_A, n, z0.at[n])
+            low = low + z0[n].astype(f32)
+            arrived(RZ_B, n, z1.at[n])
+            high = high + z1[n].astype(f32)
+        out[part, :half] = low.astype(bf16)
+        out[part, half:] = high.astype(bf16)
+
+    def drain(n, carry):
+        @pl.when((n > 0) & (n < items - 1))
+        def _():
+            left(Z_A, n, g0.at[c, n, here])
+            left(Z_B, n, g1.at[c, n, here])
+            left(RZ_A, n, d0.at[n])
+            left(RZ_B, n, d1.at[n])
+
+        left(X_A2, n, g0.at[c, n, here])
+        left(Y_B2, n, g1.at[c, n, here])
+        left(Y_A3, n, g0.at[c, n, here])
+        left(X_B3, n, g1.at[c, n, here])
+        left(Y_A4, n, g0.at[c, n, other_x])
+        left(X_B4, n, g1.at[c, n, other_y])
+        left(C_A, n, g0.at[c, n])
+        left(C_B, n, g1.at[c, n])
+        left(C_P, n, pm.at[n, 1 - c])
+        left(Y_A, n, a0.at[n, 1 - y])
+        left(X_B, n, a1.at[n, 1 - x])
+        left(X_A, n, b0.at[n, 1 - x])
+        left(Y_B, n, b1.at[n, 1 - y])
         return carry
 
-    lax.fori_loop(0, planes, drain, 0)
+    lax.fori_loop(0, items, drain, 0)
 
 
 def dense_experts(updated, ffn_in, own_routes, route_weights, gate_part, up_part, down_part):
@@ -496,36 +508,41 @@
     half = width // 2
     first = jnp.concatenate([ffn_in[:, :half], coarse, fine, spare], axis=1)
     second = ffn_in[:, half:]
-    rows = ffn_in.shape[0]
     planes = sp_count // 2
+    items = 2 * planes
+    rows = ffn_in.shape[0] // 2
     bf16 = jnp.bfloat16
     whole = pl.BlockSpec(memory_space=pltpu.VMEM)
+    far = pl.BlockSpec(memory_space=pl.ANY)
     return pl.pallas_call(
         functools.partial(experts_kernel, planes),
-        out_shape=jax.ShapeDtypeStruct((rows, width), bf16),
-        in_specs=[whole] * 6,
+        out_shape=jax.ShapeDtypeStruct((2 * rows, width), bf16),
+        in_specs=[whole] * 3 + [far] * 3,
         out_specs=whole,
         scratch_shapes=[
-            pltpu.VMEM((2, planes, 4, rows, half + 128), bf16),
-            pltpu.VMEM((2, planes, 4, rows, half), bf16),
-            pltpu.VMEM((planes, 4 * rows, width), bf16),
-            pltpu.VMEM((planes, 4 * rows, width), bf16),
-            pltpu.VMEM((planes, 4 * rows, width), bf16),
-            pltpu.VMEM((planes, 2, 2, rows, half), bf16),
-            pltpu.VMEM((planes, 2, 2, rows, half), bf16),
-            pltpu.VMEM((planes, 2, rows, half), bf16),
-            pltpu.VMEM((planes, 2, rows, half), bf16),
-            pltpu.VMEM((planes, 2, rows, half), bf16),
-            pltpu.VMEM((planes, 2, rows, half), bf16),
-            pltpu.VMEM((planes, rows, half), bf16),
-            pltpu.VMEM((planes, rows, half), bf16),
-            pltpu.VMEM((planes, rows, half), bf16),
-            pltpu.VMEM((planes, rows, half), bf16),
-            pltpu.VMEM((planes, rows, half), bf16),
-            pltpu.VMEM((planes, rows, half), bf16),
-            pltpu.SemaphoreType.DMA((17, planes)),
-            pltpu.SemaphoreType.DMA((17, planes)),
-            pltpu.SemaphoreType.DMA((2,)),
+            pltpu.VMEM(gate_part.shape, bf16),
+            pltpu.VMEM(up_part.shape, bf16),
+            pltpu.VMEM(down_part.shape, bf16),
+            pltpu.VMEM((2, items, 4, rows, half + 128), bf16),
+            pltpu.VMEM((2, items, 4, rows, half), bf16),
+            pltpu.VMEM((items, 2, 4 * rows, width), bf16),
+            pltpu.VMEM((items, 4 * rows, width), bf16),
+            pltpu.VMEM((items, 2, 2, rows, half), bf16),
+            pltpu.VMEM((items, 2, 2, rows, half), bf16),
+            pltpu.VMEM((items, 2, rows, half), bf16),
+            pltpu.VMEM((items, 2, rows, half), bf16),
+            pltpu.VMEM((items, 2, rows, half), bf16),
+            pltpu.VMEM((items, 2, rows, half), bf16),
+            pltpu.VMEM((items, rows, half), bf16),
+            pltpu.VMEM((items, rows, half), bf16),
+            pltpu.VMEM((items, rows, half), bf16),
+            pltpu.VMEM((items, rows, half), bf16),
+            pltpu.VMEM((items, rows, half), bf16),
+            pltpu.VMEM((items, rows, half), bf16),
+            pltpu.SemaphoreType.DMA((17, items)),
+            pltpu.SemaphoreType.DMA((17, items)),
+            pltpu.SemaphoreType.DMA((4,)),
+            pltpu.SemaphoreType.DMA((3,)),
         ],
         compiler_params=pltpu.CompilerParams(
             collective_id=0, has_side_effects=True, vmem_limit_bytes=63 * 1024 * 1024

time: 166 us -> 155 us (0.934)
  Pallas kernels: 151 us -> 140 us
    pallas_call x1, Pallas kernels: 105 us -> 93.9 us  [dense_experts(): pl.pallas_call(functools.partial(experts_kernel, planes), out_shape=jax.S...]
where the time goes in v1:
time: 155 us
  Pallas kernels  140 us (90%)
  local copies, waits for them, and re-layouts  8.38 us (5%)
  other arithmetic  4.08 us (3%)
  matrix products  2.73 us (2%)
    pallas_call x1, Pallas kernels, dense_experts(): pl.pallas_call(functools.partial(experts_kernel, planes), out_shape=jax.S...  93.9 us
    pallas_call x1, Pallas kernels, retention(): pl.pallas_call(functools.partial(state_kernel, planes), out_shape=jax.Sha...  25.1 us
    pallas_call x1, Pallas kernels, body(): pl.pallas_call(mix_kernel, out_shape=jax.ShapeDtypeStruct((rows_own, mode...  12.3 us
    pallas_call x1, Pallas kernels, retention(): pl.pallas_call(retention_kernel, grid=(local_heads,), out_shape=(jax.Shap...  4.35 us
    pallas_call x1, Pallas kernels, retention(): pl.pallas_call(norm_kernel, grid=(local_heads,), out_shape=jax.ShapeDtype...  3.95 us

profile of v1, /device:TPU:0, one launch (start us, length us, event | category | flops | bytes accessed | tf_op | source)
XLA Modules:
  0.0 154.9 jit_solution(5780144578635704354)
XLA Ops:
  0.0 0.5 fusion
  0.6 0.8 pad_maximum_fusion
  1.4 0.7 reshape.49
  2.1 1.2 reduce-window.6
  3.4 0.1 copy.30
  3.6 0.1 copy.31
  3.7 0.8 copy.32
  4.5 4.3 %shard_map.136 = (f32[256,512]{1,0:T(8,128)}, bf16[256,512]{1,0:T(8,128)(2,1)}, f32[4,136,128]{2,1,0:T(8,128)}) custom-call(bf16[256,512]{1,0:T(8,128)(2,1)} %q_ref.1, bf16[256,512]{1,0:T(8,128)(2,1)} %k_ref.1, bf16[256,512]{1,0:T(8,128)(2,1)} %v_ref.1, f32[256,128]{1,0:T(8,128)} %get-tuple-element.18.cos_ref, f32[256,128]{1,0:T(8,128)} %get-tuple-element.19.sin_ref, ...), custom_call_target="tpu_custom_call" | custom-call | tf_op jit(solution)/shard_map/pallas_call | solution.py:212
  8.9 1.6 %slice.31.state = bf16[4,128,128]{2,1,0:T(8,128)(2,1)} slice(f32[4,136,128]{2,1,0:T(8,128)} %get-tuple-element.10), slice={[0:4], [0:128], [0:128]} | slice | bytes 262144 | tf_op jit(solution)/shard_map/slice | solution.py:253
  10.5 0.8 slice_reduce_fusion
  11.3 0.6 pad.7.totals
  12.0 25.1 %shard_map.137.enter_ref = bf16[4,128,128]{2,1,0:T(8,128)(2,1)} custom-call(bf16[4,128,128]{2,1,0:T(8,128)(2,1)} %slice.31.state, f32[8,128]{1,0:T(8,128)} %pad.7.totals), custom_call_target="tpu_custom_call" | custom-call | tf_op jit(solution)/shard_map/pallas_call | solution.py:240
  37.1 3.9 %shard_map.138 = bf16[256,512]{1,0:T(8,128)(2,1)} custom-call(f32[256,512]{1,0:T(8,128)} %get-tuple-element.8.ret_ref, bf16[256,512]{1,0:T(8,128)(2,1)} %get-tuple-element.9.qdec_ref, bf16[4,128,128]{2,1,0:T(8,128)(2,1)} %shard_map.137.enter_ref, f32[1,512]{1,0:T(1,128)} %bitcast.21, bf16[256,512]{1,0:T(8,128)(2,1)} %gate_ref.1), custom_call_target="tpu_custom_call" | custom-call | tf_op jit(solution)/shard_map/pallas_call | solution.py:262
  41.1 2.7 %convolution_convert_fusion = bf16[256,2048]{1,0:T(8,128)(2,1)} fusion(bf16[256,512]{1,0:T(8,128)(2,1)} %shard_map.138, bf16[512,2048]{1,0:T(8,128)(2,1)S(1)} %copy-done.2), kind=kOutput, calls=%fused_computation | convolution fusion | flops 537395200 | bytes 3407872 | tf_op jit(solution)/shard_map/dot_general | solution.py:577
  43.8 12.3 %shard_map.139 = f32[64,2048]{1,0:T(8,128)} custom-call(bf16[2,2,64,2048]{3,2,1,0:T(8,128)(2,1)} %bitcast.13), custom_call_target="tpu_custom_call" | custom-call | tf_op jit(solution)/shard_map/pallas_call | solution.py:579
  56.1 1.2 multiply_reduce_fusion
  57.4 0.1 multiply_convert_fusion
  57.5 0.7 fusion.1
  58.3 0.1 copy.34
  58.4 0.1 copy.33
  58.4 0.1 copy.35
  58.6 0.8 concatenate.11.x0
  59.3 93.9 %shard_map.140 = bf16[64,2048]{1,0:T(8,128)(2,1)} custom-call(bf16[64,1152]{1,0:T(8,128)(2,1)} %concatenate.11.x0, bf16[64,1024]{1,0:T(8,128)(2,1)} %get-tuple-element.13.x1, f32[64,2048]{1,0:T(8,128)} %copy-done.1, bf16[2048,512]{1,0:T(8,128)(2,1)} %bitcast.14, bf16[2048,512]{1,0:T(8,128)(2,1)} %bitcast.15, bf16[512,2048]{1,0:T(8,128)(2,1)} %bitcast.16), custom_call_target="tpu_custom_call" | custom-call | tf_op jit(solution)/shard_map/pallas_call | solution.py:517
  153.2 1.7 %copy.37 = bf16[64,2048]{1,0:T(8,128)(2,1)} copy(bf16[64,2048]{1,0:T(8,128)(2,1)} %shard_map.140) | data formatting | bytes 524288
  (27 shorter events, 0.3 us)
Async XLA Ops:
  0.0 58.2 %copy-start = (s32[256,4]{0,1:T(4,128)S(1)}, s32[256,4]{0,1:T(4,128)}, u32[]{:S(2)}) copy-start(s32[256,4]{0,1:T(4,128)} %param.26) | copy-start | bytes 12292
  0.6 40.5 %copy-start.2 = (bf16[512,2048]{1,0:T(8,128)(2,1)S(1)}, bf16[512,2048]{1,0:T(8,128)(2,1)}, u32[]{:S(2)}) copy-start(bf16[512,2048]{1,0:T(8,128)(2,1)} %param.20) | copy-start | bytes 6291460
  3.7 0.8 copy-start.4
  41.1 15.0 %copy-start.3 = (bf16[64,2048]{1,0:T(8,128)(2,1)S(1)}, bf16[64,2048]{1,0:T(8,128)(2,1)}, u32[]{:S(2)}) copy-start(bf16[64,2048]{1,0:T(8,128)(2,1)} %param.21) | copy-start | bytes 786436
  43.8 13.5 %copy-start.5 = (f32[2048]{0:T(1024)S(1)}, f32[2048]{0:T(1024)}, u32[]{:S(2)}) copy-start(f32[2048]{0:T(1024)} %param.22) | copy-start | bytes 24580
  43.8 14.4 %copy-start.6 = (f32[64,4]{0,1:T(4,128)S(1)}, f32[64,4]{0,1:T(4,128)}, u32[]{:S(2)}) copy-start(f32[64,4]{0,1:T(4,128)} %param.27) | copy-start | bytes 3076
  57.3 2.0 %copy-start.1 = (f32[64,2048]{1,0:T(8,128)}, f32[64,2048]{1,0:T(8,128)S(1)}, u32[]{:S(2)}) copy-start(f32[64,2048]{1,0:T(8,128)S(1)} %get-tuple-element.12.upd) | copy-start | bytes 1572868

commit v2 on v1

v2 whole, which is shorter than its diff:
```python
import functools

import jax
import jax.numpy as jnp
import numpy as np
from jax import lax
from jax.experimental import pallas as pl
from jax.experimental.pallas import tpu as pltpu
from jax.sharding import PartitionSpec as P

HEAD_DIM = 128
TOPK = 4
BLOCK = 128


highest = lax.Precision.HIGHEST
rope_base = 10000.0
group_eps = 1e-05
square_eps = 1e-06
clamp_limit = 7.0
swish_alpha = 1.702


def rotary_angles(positions, head_dim):
    half_dim = head_dim // 2
    inverse = rope_base ** (-jnp.arange(half_dim, dtype=jnp.float32) / half_dim)
    return positions[:, None] * inverse[None, :]


def square_norm(updated, gain_row):
    factor = lax.rsqrt(jnp.mean(updated * updated, axis=-1, keepdims=True) + square_eps)
    return (updated * factor * gain_row).astype(jnp.bfloat16)


def expert_rows(rows, gate_part, up_part):
    gate_pre = jnp.dot(rows, gate_part, preferred_element_type=jnp.float32)
    up_pre = jnp.dot(rows, up_part, preferred_element_type=jnp.float32)
    gate_clip = jnp.minimum(gate_pre, clamp_limit)
    up_clip = jnp.clip(up_pre, -clamp_limit, clamp_limit)
    return ((up_clip + 1.0) * (gate_clip * jax.nn.sigmoid(gate_clip * swish_alpha))).astype(
        jnp.bfloat16
    )


def slot_ranks(route_block, experts):
    flat_routes = route_block.reshape(-1)
    onehot = (flat_routes[:, None] == jnp.arange(experts, dtype=jnp.int32)[None, :]).astype(
        jnp.int32
    )
    return (flat_routes, jnp.sum(jnp.cumsum(onehot, axis=0) * onehot, axis=1) - 1)


def retention_kernel(q_ref, k_ref, v_ref, cos_ref, sin_ref, cum_ref, cum_row_ref, ret_ref, qdec_ref, state_ref):
    head = pl.program_id(0)
    length = q_ref.shape[0]
    cosine, sine = cos_ref[...], sin_ref[...]
    half = HEAD_DIM // 2

    def turned(ref):
        rows = ref[...].astype(jnp.float32)
        return rows * cosine + pltpu.roll(rows, half, 1) * sine

    lanes = lax.broadcasted_iota(jnp.int32, cum_ref.shape, 1)
    column = jnp.sum(jnp.where(lanes == head, cum_ref[...], 0.0), axis=1, keepdims=True)
    row = cum_row_ref[0]
    queries = turned(q_ref)
    keys = turned(k_ref) * HEAD_DIM ** (-0.5)
    values = v_ref[...]
    scores = lax.dot_general(
        queries.astype(jnp.bfloat16),
        keys.astype(jnp.bfloat16),
        (((1,), (1,)), ((), ())),
        preferred_element_type=jnp.float32,
    )
    causal = lax.broadcasted_iota(jnp.int32, (length, length), 0) >= lax.broadcasted_iota(
        jnp.int32, (length, length), 1
    )
    weights = jnp.where(causal, jnp.exp(jnp.minimum(column - row, 0.0)), 0.0)
    ret_ref[...] = jnp.dot(
        (scores * weights).astype(jnp.bfloat16), values, preferred_element_type=jnp.float32
    )
    qdec_ref[...] = (queries * jnp.exp(column)).astype(jnp.bfloat16)
    total = column[length - 1 :, :]
    tailed = (keys * jnp.exp(total - column)).astype(jnp.bfloat16)
    state_ref[0, :HEAD_DIM, :] = lax.dot_general(
        tailed, values, (((0,), (0,)), ((), ())), preferred_element_type=jnp.float32
    )
    state_ref[0, HEAD_DIM:, :] = jnp.broadcast_to(total, (8, HEAD_DIM))


def norm_kernel(ret_ref, qdec_ref, enter_ref, gain_ref, gate_ref, hidden_ref):
    retained = ret_ref[...] + jnp.dot(
        qdec_ref[...], enter_ref[0].astype(jnp.bfloat16), preferred_element_type=jnp.float32
    )
    centred = retained - jnp.mean(retained, axis=-1, keepdims=True)
    variance = jnp.mean(centred * centred, axis=-1, keepdims=True)
    gate = gate_ref[...].astype(jnp.float32)
    scaled = centred * lax.rsqrt(variance + group_eps) * gain_ref[...]
    hidden_ref[...] = (scaled * (gate / (1.0 + jnp.exp(-gate)))).astype(jnp.bfloat16)


def retention(query_rows, key_rows, value_rows, gate_rows, log_decay, head_gain):
    length, local_heads = log_decay.shape
    width = query_rows.shape[1]
    sp_count, mine = lax.axis_size("sp"), lax.axis_index("sp")
    positions = (mine * length + jnp.arange(length, dtype=jnp.int32)).astype(jnp.float32)
    angles = rotary_angles(positions, HEAD_DIM)
    cosine, sine = jnp.cos(angles), jnp.sin(angles)
    cosine = jnp.concatenate([cosine, cosine], axis=1)
    sine = jnp.concatenate([-sine, sine], axis=1)
    cumulative = jnp.cumsum(log_decay, axis=0)
    rows_spec = pl.BlockSpec((length, HEAD_DIM), lambda h: (0, h))
    table_spec = pl.BlockSpec((length, HEAD_DIM), lambda h: (0, 0))
    retained, qdec, state = pl.pallas_call(
        retention_kernel,
        grid=(local_heads,),
        out_shape=(
            jax.ShapeDtypeStruct((length, width), jnp.float32),
            jax.ShapeDtypeStruct((length, width), jnp.bfloat16),
            jax.ShapeDtypeStruct((local_heads, HEAD_DIM + 8, HEAD_DIM), jnp.float32),
        ),
        in_specs=[
            rows_spec,
            rows_spec,
            rows_spec,
            table_spec,
            table_spec,
            pl.BlockSpec((length, local_heads), lambda h: (0, 0)),
            pl.BlockSpec((1, 1, length), lambda h: (h, 0, 0)),
        ],
        out_specs=(
            rows_spec,
            rows_spec,
            pl.BlockSpec((1, HEAD_DIM + 8, HEAD_DIM), lambda h: (h, 0, 0)),
        ),
    )(query_rows, key_rows, value_rows, cosine, sine, cumulative, cumulative.T[:, None, :])
    pieces = lax.all_gather(state, "sp")
    totals = pieces[:, :, HEAD_DIM, 0]
    index = jnp.arange(sp_count, dtype=jnp.int32)
    between = (index[None, :] > index[:, None]) & (index[None, :] < mine)
    gap = jnp.sum(jnp.where(between[:, :, None], totals[None], 0.0), axis=1)
    factor = jnp.where((index < mine)[:, None], jnp.exp(gap), 0.0)
    entering = jnp.sum(factor[:, :, None, None] * pieces[:, :, :HEAD_DIM, :], axis=0)
    return pl.pallas_call(
        norm_kernel,
        grid=(local_heads,),
        out_shape=jax.ShapeDtypeStruct((length, width), jnp.bfloat16),
        in_specs=[
            rows_spec,
            rows_spec,
            pl.BlockSpec((1, HEAD_DIM, HEAD_DIM), lambda h: (h, 0, 0)),
            pl.BlockSpec((1, HEAD_DIM), lambda h: (0, h)),
            rows_spec,
        ],
        out_specs=rows_spec,
    )(retained, qdec, entering, head_gain[None, :], gate_rows)


(
    UP_A, UP_B, DOWN_A, DOWN_B, X_A2, Y_B2, Y_A3, Y_A4, X_B3, X_B4, C_A, C_B, C_P, Y_A, X_B, X_A, Y_B, RZ_A, RZ_B,
    TOTAL, CHAIN, ACROSS, MIX_C, MIX_Y,
) = range(24)


def layer_kernel(
    planes, q_ref, k_ref, v_ref, gate_ref, logs, head_gain, near_table, base_table, residual, ffn_gain, shares,
    wo_hbm, wg_hbm, wu_hbm, wd_hbm, out,
    wo, wg, wu, wd, rotary, turned_k, ret, qdec, state, cum_col, cum_row, total_own, total_x, carry_in, carry_out,
    side_out, side_in, hidden, blend, from_core, held, from_y, upd,
    g0, g1, pm, pr, a0, a1, r10, r11, b0, b1, r20, r21, d0, d1, z0, z1,
    ssem, rsem, wsem,
):
    sp, tp = lax.axis_index("sp"), lax.axis_index("tp")
    sp_count = 2 * planes
    z, x = sp // 2, sp % 2
    y, c = tp // 2, tp % 2
    own_rows, width = out.shape
    half = width // 2
    rows = own_rows // 2
    items = 2 * planes
    lag = items - 3
    f32, bf16 = jnp.float32, jnp.bfloat16
    to_core = {"sp": sp, "tp": y * 2 + (1 - c)}
    to_y = {"sp": sp, "tp": (1 - y) * 2 + c}
    to_x = {"sp": z * 2 + (1 - x), "tp": tp}

    def half_of(n):
        return jnp.where(n == items - 1, 1, jnp.where(n == 0, 0, (n + 1) % 2))

    def plane_at(k):
        low = z < planes // 2
        mirrored = jnp.where(low, z, planes - 1 - z)
        q = jnp.where(k <= mirrored, mirrored - k, k)
        return jnp.where(low, q, planes - 1 - q)

    def plane_of(n):
        return plane_at(((n + 1) // 2) % planes)

    def item_of(n):
        return 2 * plane_of(n) + half_of(n)

    def step_of(turn):
        back = items - 3 - 2 * ((turn - 1) // 2) + (turn - 1) % 2
        return jnp.where((turn == 0) | (turn == items - 1), turn, back)

    def turn_at(u):
        return jnp.where(u == 0, 0, u - 1)

    def has_turn(u):
        return (u == 0) | ((u >= 2) & (u <= items))

    def at_plane(p):
        return {"sp": p * 2 + x, "tp": tp}

    def to_z(i):
        return at_plane((z + planes - i) % planes)

    def move(kind, n, src, dst, device, m=None):
        return pltpu.make_async_remote_copy(
            src_ref=src, dst_ref=dst, send_sem=ssem.at[kind, n],
            recv_sem=rsem.at[kind, n if m is None else m],
            device_id=device, device_id_type=pl.DeviceIdType.MESH,
        )

    def send(kind, n, src, dst, device, m=None):
        move(kind, n, src, dst, device, m).start()

    def arrived(kind, n, dst):
        move(kind, n, dst, dst, to_core).wait_recv()

    def left(kind, n, src):
        move(kind, n, src, src, to_core).wait_send()

    barrier = pltpu.get_barrier_semaphore()
    for device in [to_core, to_y, to_x] + [to_z(i) for i in range(1, planes)]:
        pl.semaphore_signal(barrier, inc=1, device_id=device, device_id_type=pl.DeviceIdType.MESH)

    weights = [
        pltpu.make_async_copy(wo_hbm, wo, wsem.at[0]),
        pltpu.make_async_copy(wg_hbm, wg, wsem.at[1]),
        pltpu.make_async_copy(wu_hbm, wu, wsem.at[2]),
        pltpu.make_async_copy(wd_hbm, wd, wsem.at[3]),
    ]
    for copy in weights:
        copy.start()

    length = q_ref.shape[0]
    heads = state.shape[0]
    dim = HEAD_DIM
    after = lax.broadcasted_iota(jnp.int32, (length, length), 0) >= lax.broadcasted_iota(
        jnp.int32, (length, length), 1
    )
    ones = jnp.where(after, 1.0, 0.0).astype(f32)
    log_rows = jnp.concatenate([logs[...], jnp.zeros((8 - heads, length), f32)], axis=0)
    cum_row[...] = lax.dot_general(
        log_rows, ones, (((1,), (1,)), ((), ())), precision=highest, preferred_element_type=f32
    )
    cum_col[...] = lax.dot_general(
        ones, log_rows, (((1,), (1,)), ((), ())), precision=highest, preferred_element_type=f32
    )
    total_own[...] = jnp.broadcast_to(cum_row[:, length - 1 :], (8, dim))
    pl.semaphore_wait(barrier, 2 + planes)
    send(TOTAL, 0, total_own, total_x, to_x)

    base = base_table[pl.ds(sp * 8, 8), :]
    cosine = base[0:1] * near_table[0] - base[1:2] * near_table[1]
    sine = base[2:3] * near_table[0] + base[3:4] * near_table[1]
    rotary[0] = cosine
    rotary[1] = sine

    def turned(rows_in):
        wide = rows_in.astype(f32)
        return wide * rotary[0] + pltpu.roll(wide, dim // 2, 1) * rotary[1]

    def column_of(h):
        lanes = lax.broadcasted_iota(jnp.int32, cum_col.shape, 1)
        return jnp.sum(jnp.where(lanes == h, cum_col[...], 0.0), axis=1, keepdims=True)

    for h in range(heads):
        lanes = pl.ds(h * dim, dim)
        keys = turned(k_ref[:, lanes]) * dim ** (-0.5)
        turned_k[:, lanes] = keys.astype(bf16)
        column = column_of(h)
        tailed = (keys * jnp.exp(column[length - 1 :, :] - column)).astype(bf16)
        state[h] = lax.dot_general(
            tailed, v_ref[:, lanes], (((0,), (0,)), ((), ())), preferred_element_type=f32
        )

    def attend(h, carry):
        lanes = pl.ds(pl.multiple_of(h * dim, dim), dim)
        queries = turned(q_ref[:, lanes])
        column = column_of(h)
        scores = lax.dot_general(
            queries.astype(bf16), turned_k[:, lanes], (((1,), (1,)), ((), ())), preferred_element_type=f32
        )
        gap = jnp.minimum(column - cum_row[pl.ds(h, 1), :], 0.0)
        decays = jnp.where(after, jnp.exp(gap), 0.0)
        ret[:, lanes] = jnp.dot((scores * decays).astype(bf16), v_ref[:, lanes], preferred_element_type=f32)
        qdec[:, lanes] = (queries * jnp.exp(column)).astype(bf16)
        return carry

    early = jnp.where(z >= planes // 2, heads, 0)
    lax.fori_loop(0, early, attend, 0)

    arrived(TOTAL, 0, total_x)
    left_side = x == 0
    for h in range(heads):
        own_total, x_total = total_own[h : h + 1, :], total_x[h : h + 1, :]

        @pl.when(z > 0)
        def _():
            arrived(CHAIN, h, carry_in.at[h])

        @pl.when(z == 0)
        def _():
            carry_in[h] = jnp.zeros((dim, dim), bf16)

        before = carry_in[h].astype(f32)

        @pl.when(z + 1 < planes)
        def _():
            fresh = jnp.where(left_side, jnp.exp(x_total), 1.0) * state[h]
            carry_out[h] = (jnp.exp(own_total + x_total) * before + fresh).astype(bf16)
            send(CHAIN, h, carry_out.at[h], carry_in.at[h], at_plane(z + 1))

        side_out[h] = jnp.where(left_side, jnp.exp(own_total) * before + state[h], before).astype(bf16)
        send(ACROSS, h, side_out.at[h], side_in.at[h], to_x)

    lax.fori_loop(early, heads, attend, 0)

    for h in range(heads):
        lanes = pl.ds(h * dim, dim)
        arrived(ACROSS, h, side_in.at[h])
        factor = jnp.where(left_side, 1.0, jnp.exp(total_x[h : h + 1, :]))
        entering = (factor * carry_in[h].astype(f32) + side_in[h].astype(f32)).astype(bf16)
        retained = ret[:, lanes] + jnp.dot(qdec[:, lanes], entering, preferred_element_type=f32)
        centred = retained - jnp.mean(retained, axis=-1, keepdims=True)
        variance = jnp.mean(centred * centred, axis=-1, keepdims=True)
        gate_in = gate_ref[:, lanes].astype(f32)
        scaled = centred * lax.rsqrt(variance + group_eps) * head_gain[:, lanes]
        hidden[:, lanes] = (scaled * (gate_in / (1.0 + jnp.exp(-gate_in)))).astype(bf16)

    weights[0].wait()
    pieces = blend.shape[0]
    span = width // pieces

    def cross(j):
        arrived(MIX_C, j, from_core.at[j])
        held[j] = (blend[j, c, 1 - y].astype(f32) + from_core[j, 1 - y].astype(f32)).astype(bf16)
        send(MIX_Y, j, held.at[j], from_y.at[j], to_y)

    for j in range(pieces):
        mixed = jnp.dot(hidden[...], wo[:, pl.ds(j * span, span)], preferred_element_type=f32).astype(bf16)
        for q in range(4):
            blend[j, q % 2, q // 2] = mixed[q * own_rows : (q + 1) * own_rows, :]
        send(MIX_C, j, blend.at[j, 1 - c], from_core.at[j], to_core)
        if j > 0:
            cross(j - 1)
    cross(pieces - 1)
    square = jnp.zeros((own_rows, 1), f32)
    for j in range(pieces):
        cols = pl.ds(j * span, span)
        base_rows = residual[:, cols].astype(f32) + blend[j, c, y].astype(f32) + from_core[j, y].astype(f32)
        arrived(MIX_Y, j, from_y.at[j])
        total = base_rows + from_y[j].astype(f32)
        upd[:, cols] = total
        square = square + jnp.sum(total * total, axis=-1, keepdims=True)
    scale = lax.rsqrt(square * (1.0 / width) + square_eps)

    here = x * 2 + y
    other_x = (1 - x) * 2 + y
    other_y = x * 2 + (1 - y)
    other_xy = (1 - x) * 2 + (1 - y)
    share = jnp.transpose(shares[...])[:own_rows, :]
    coarse = share.astype(bf16).astype(f32)
    tail_rows = (coarse + pltpu.roll(share - coarse, sp_count, 1)).astype(bf16)
    for r in range(2):
        mine, n = slice(r * rows, (r + 1) * rows), 2 * z + r
        ready = (upd[mine, :] * scale[mine] * ffn_gain[...]).astype(bf16)
        g0[c, n, here, :, :half] = ready[:, :half]
        g0[c, n, here, :, half:] = tail_rows[mine]
        g1[c, n, here] = ready[:, half:]

    def spread(n):
        send(X_A2, n, g0.at[c, n, here], g0.at[c, n, here], to_x)
        send(Y_B2, n, g1.at[c, n, here], g1.at[c, n, here], to_y)
        send(Y_A3, n, g0.at[c, n, here], g0.at[c, n, here], to_y)
        send(X_B3, n, g1.at[c, n, here], g1.at[c, n, here], to_x)

    def raise_up(n):
        @pl.when(z + 1 < planes)
        def _():
            send(UP_A, n, g0.at[c, n, here], g0.at[c, n, here], at_plane(z + 1))
            send(UP_B, n, g1.at[c, n, here], g1.at[c, n, here], at_plane(z + 1))

    def hand_down(n):
        @pl.when(z > 0)
        def _():
            send(DOWN_A, n, g0.at[c, n, here], g0.at[c, n, here], at_plane(z - 1))
            send(DOWN_B, n, g1.at[c, n, here], g1.at[c, n, here], at_plane(z - 1))

    spread(2 * z)
    for r in range(2):
        raise_up(2 * z + r)
        hand_down(2 * z + r)

    def tick(t, carry):
        def relay():
            n = item_of(t)
            arrived(X_A2, n, g0.at[c, n, other_x])
            send(Y_A4, n, g0.at[c, n, other_x], g0.at[c, n, other_x], to_y)
            arrived(Y_B2, n, g1.at[c, n, other_y])
            send(X_B4, n, g1.at[c, n, other_y], g1.at[c, n, other_y], to_x)

        pl.when(t == 0)(relay)

        @pl.when(t + 1 < items)
        def _():
            k, r = (t + 2) // 2, t % 2

            @pl.when((t + 1 < items - 1) & (z - k >= 0))
            def _():
                n = 2 * (z - k) + r
                arrived(UP_A, n, g0.at[c, n, here])
                arrived(UP_B, n, g1.at[c, n, here])
                raise_up(n)

            @pl.when((t + 1 < items - 1) & (z + k < planes))
            def _():
                n = 2 * (z + k) + r
                arrived(DOWN_A, n, g0.at[c, n, here])
                arrived(DOWN_B, n, g1.at[c, n, here])
                hand_down(n)

            spread(item_of(t + 1))

        pl.when((t > 0) & (t < items))(relay)

        @pl.when(t == 2)
        def _():
            for copy in weights[1:]:
                copy.wait()

        @pl.when((t >= 2) & (t < items + 2))
        def _():
            n = item_of(t - 2)
            arrived(C_A, n, g0.at[1 - c, n])
            arrived(C_B, n, g1.at[1 - c, n])
            lead = g0[:, n].reshape(8 * rows, half + 128)
            tail = lead[:, half:].astype(f32)
            lead = lead[:, :half]
            rest = g1[:, n].reshape(8 * rows, half)
            lane = lax.broadcasted_iota(jnp.int32, tail.shape, 1)
            weight = jnp.sum(
                jnp.where((lane == sp) | (lane == sp + sp_count), tail, 0.0), axis=1, keepdims=True
            )

            def product(w):
                return jnp.dot(lead, w[:half, :], preferred_element_type=f32) + jnp.dot(
                    rest, w[half:, :], preferred_element_type=f32
                )

            gate = jnp.minimum(product(wg), clamp_limit)
            up = jnp.clip(product(wu), -clamp_limit, clamp_limit)
            act = ((up + 1.0) * (gate / (1.0 + jnp.exp(-swish_alpha * gate)))).astype(bf16)
            made = (jnp.dot(act, wd[...], preferred_element_type=f32) * weight).astype(bf16)
            pm[n] = made.reshape(2, 4 * rows, 2 * half)
            send(C_P, n, pm.at[n, 1 - c], pr.at[n], to_core)

        @pl.when((t >= 1) & (t < items + 1))
        def _():
            n = item_of(t - 1)
            arrived(Y_A3, n, g0.at[c, n, other_y])
            arrived(Y_A4, n, g0.at[c, n, other_xy])
            arrived(X_B3, n, g1.at[c, n, other_x])
            arrived(X_B4, n, g1.at[c, n, other_xy])
            send(C_A, n, g0.at[c, n], g0.at[c, n], to_core)
            send(C_B, n, g1.at[c, n], g1.at[c, n], to_core)

        @pl.when(has_turn(t - lag))
        def _():
            n = item_of(step_of(turn_at(t - lag)))
            arrived(C_P, n, pr.at[n])
            for q in range(4):
                part = pl.ds(q * rows, rows)
                total = (pm[n, c, part, :].astype(f32) + pr[n, part, :].astype(f32)).astype(bf16)
                a0[n, q % 2, q // 2] = total[:, :half]
                a1[n, q // 2, q % 2] = total[:, half:]
            send(Y_A, n, a0.at[n, 1 - y], r10.at[n], to_y)
            send(X_B, n, a1.at[n, 1 - x], r11.at[n], to_x)

        @pl.when(has_turn(t - lag - 1))
        def _():
            n = item_of(step_of(turn_at(t - lag - 1)))
            arrived(Y_A, n, r10.at[n])
            b0[n] = (a0[n, y].astype(f32) + r10[n].astype(f32)).astype(bf16)
            send(X_A, n, b0.at[n, 1 - x], r20.at[n], to_x)
            arrived(X_B, n, r11.at[n])
            b1[n] = (a1[n, x].astype(f32) + r11[n].astype(f32)).astype(bf16)
            send(Y_B, n, b1.at[n, 1 - y], r21.at[n], to_y)

        @pl.when(has_turn(t - lag - 2))
        def _():
            turn = step_of(turn_at(t - lag - 2))
            n = item_of(turn)
            arrived(X_A, n, r20.at[n])
            d0[n] = (b0[n, x].astype(f32) + r20[n].astype(f32)).astype(bf16)
            arrived(Y_B, n, r21.at[n])
            d1[n] = (b1[n, y].astype(f32) + r21[n].astype(f32)).astype(bf16)

            @pl.when((turn > 0) & (turn < items - 1))
            def _():
                m = 2 * z + half_of(turn)
                send(RZ_A, n, d0.at[n], z0.at[m], at_plane(plane_of(turn)), m)
                send(RZ_B, n, d1.at[n], z1.at[m], at_plane(plane_of(turn)), m)

        return carry

    lax.fori_loop(0, items + lag + 3, tick, 0)
    for r in range(2):
        n, part = 2 * z + r, pl.ds(r * rows, rows)
        low = upd[part, :half] + d0[n].astype(f32)
        high = upd[part, half:] + d1[n].astype(f32)
        for i in range(1, planes):
            n = 2 * ((z + i) % planes) + r
            arrived(RZ_A, n, z0.at[n])
            low = low + z0[n].astype(f32)
            arrived(RZ_B, n, z1.at[n])
            high = high + z1[n].astype(f32)
        out[part, :half] = low.astype(bf16)
        out[part, half:] = high.astype(bf16)

    def drain(n, carry):
        p = n // 2

        @pl.when((p <= z) & (z + 1 < planes))
        def _():
            left(UP_A, n, g0.at[c, n, here])
            left(UP_B, n, g1.at[c, n, here])

        @pl.when((p >= z) & (z > 0))
        def _():
            left(DOWN_A, n, g0.at[c, n, here])
            left(DOWN_B, n, g1.at[c, n, here])

        @pl.when((p < z) | (p > z))
        def _():
            left(RZ_A, n, d0.at[n])
            left(RZ_B, n, d1.at[n])

        left(X_A2, n, g0.at[c, n, here])
        left(Y_B2, n, g1.at[c, n, here])
        left(Y_A3, n, g0.at[c, n, here])
        left(X_B3, n, g1.at[c, n, here])
        left(Y_A4, n, g0.at[c, n, other_x])
        left(X_B4, n, g1.at[c, n, other_y])
        left(C_A, n, g0.at[c, n])
        left(C_B, n, g1.at[c, n])
        left(C_P, n, pm.at[n, 1 - c])
        left(Y_A, n, a0.at[n, 1 - y])
        left(X_B, n, a1.at[n, 1 - x])
        left(X_A, n, b0.at[n, 1 - x])
        left(Y_B, n, b1.at[n, 1 - y])
        return carry

    lax.fori_loop(0, items, drain, 0)
    left(TOTAL, 0, total_own)
    for h in range(heads):
        left(ACROSS, h, side_out.at[h])

        @pl.when(z + 1 < planes)
        def _():
            left(CHAIN, h, carry_out.at[h])

    for j in range(pieces):
        left(MIX_C, j, blend.at[j, 1 - c])
        left(MIX_Y, j, held.at[j])


def rope_tables(length, spans):
    half_dim = HEAD_DIM // 2
    rates = rope_base ** (-np.arange(half_dim, dtype=np.float64) / half_dim)
    rates = np.concatenate([rates, rates])[None, :]
    near = np.arange(length, dtype=np.float64)[:, None] * rates
    starts = (np.arange(spans, dtype=np.float64) * length)[:, None] * rates
    sign = np.concatenate([-np.ones(half_dim), np.ones(half_dim)])[None, :]
    base = np.zeros((spans, 8, HEAD_DIM))
    base[:, 0], base[:, 1] = np.cos(starts), np.sin(starts)
    base[:, 2], base[:, 3] = sign * np.sin(starts), sign * np.cos(starts)
    near_table = np.stack([np.cos(near), np.sin(near)]).astype(np.float32)
    return jnp.asarray(near_table), jnp.asarray(base.reshape(spans * 8, HEAD_DIM).astype(np.float32))


def fused_layer(
    query_rows, key_rows, value_rows, gate_rows, log_decay, head_gain, out_weight, residual, ffn_gain,
    gate_part, up_part, down_part, own_routes, route_weights,
):
    sp_count = lax.axis_size("sp")
    length, heads = log_decay.shape
    rows_all, width = residual.shape
    inner = query_rows.shape[1]
    chosen = own_routes.T[:, None, :] == jnp.arange(128, dtype=jnp.int32)[None, :, None]
    shares = jnp.sum(jnp.where(chosen, route_weights.T[:, None, :], 0.0), axis=0)
    shares = jnp.pad(shares, ((0, 0), (0, 128 - rows_all)))
    near_table, base_table = rope_tables(length, sp_count)
    half = width // 2
    planes = sp_count // 2
    items = 2 * planes
    rows = rows_all // 2
    pieces = 4
    span = width // pieces
    bf16, f32 = jnp.bfloat16, jnp.float32
    whole = pl.BlockSpec(memory_space=pltpu.VMEM)
    far = pl.BlockSpec(memory_space=pl.ANY)
    square = (heads, HEAD_DIM, HEAD_DIM)
    return pl.pallas_call(
        functools.partial(layer_kernel, planes),
        out_shape=jax.ShapeDtypeStruct((rows_all, width), bf16),
        in_specs=[whole] * 11 + [far] * 4,
        out_specs=whole,
        scratch_shapes=[
            pltpu.VMEM(out_weight.shape, bf16),
            pltpu.VMEM(gate_part.shape, bf16),
            pltpu.VMEM(up_part.shape, bf16),
            pltpu.VMEM(down_part.shape, bf16),
            pltpu.VMEM((2, length, HEAD_DIM), f32),
            pltpu.VMEM((length, inner), bf16),
            pltpu.VMEM((length, inner), f32),
            pltpu.VMEM((length, inner), bf16),
            pltpu.VMEM(square, f32),
            pltpu.VMEM((length, 8), f32),
            pltpu.VMEM((8, length), f32),
            pltpu.VMEM((8, HEAD_DIM), f32),
            pltpu.VMEM((8, HEAD_DIM), f32),
            pltpu.VMEM(square, bf16),
            pltpu.VMEM(square, bf16),
            pltpu.VMEM(square, bf16),
            pltpu.VMEM(square, bf16),
            pltpu.VMEM((length, inner), bf16),
            pltpu.VMEM((pieces, 2, 2, rows_all, span), bf16),
            pltpu.VMEM((pieces, 2, rows_all, span), bf16),
            pltpu.VMEM((pieces, rows_all, span), bf16),
            pltpu.VMEM((pieces, rows_all, span), bf16),
            pltpu.VMEM((rows_all, width), f32),
            pltpu.VMEM((2, items, 4, rows, half + 128), bf16),
            pltpu.VMEM((2, items, 4, rows, half), bf16),
            pltpu.VMEM((items, 2, 4 * rows, width), bf16),
            pltpu.VMEM((items, 4 * rows, width), bf16),
            pltpu.VMEM((items, 2, 2, rows, half), bf16),
            pltpu.VMEM((items, 2, 2, rows, half), bf16),
            pltpu.VMEM((items, 2, rows, half), bf16),
            pltpu.VMEM((items, 2, rows, half), bf16),
            pltpu.VMEM((items, 2, rows, half), bf16),
            pltpu.VMEM((items, 2, rows, half), bf16),
            pltpu.VMEM((items, rows, half), bf16),
            pltpu.VMEM((items, rows, half), bf16),
            pltpu.VMEM((items, rows, half), bf16),
            pltpu.VMEM((items, rows, half), bf16),
            pltpu.VMEM((items, rows, half), bf16),
            pltpu.VMEM((items, rows, half), bf16),
            pltpu.SemaphoreType.DMA((24, max(items, heads))),
            pltpu.SemaphoreType.DMA((24, max(items, heads))),
            pltpu.SemaphoreType.DMA((4,)),
        ],
        compiler_params=pltpu.CompilerParams(
            collective_id=0, has_side_effects=True, vmem_limit_bytes=63 * 1024 * 1024
        ),
    )(
        query_rows, key_rows, value_rows, gate_rows, log_decay.T, head_gain[None, :], near_table, base_table,
        residual, ffn_gain[None, :], shares, out_weight, gate_part, up_part, down_part,
    )


def body(
    query_rows,
    key_rows,
    value_rows,
    gate_rows,
    log_decay,
    head_gain,
    out_weight,
    residual,
    ffn_gain,
    gate_weight,
    up_weight,
    down_weight,
    routes,
    route_weights,
):
    tok_count = query_rows.shape[0]
    local_heads = log_decay.shape[1]
    sp_count = lax.axis_size("sp")
    tp_count = lax.axis_size("tp")
    model_width = residual.shape[1]
    rows_own = tok_count // tp_count
    capacity = max(2, 3 * rows_own * TOPK // (2 * sp_count))
    tp_index = lax.axis_index("tp")
    own_routes = lax.dynamic_slice_in_dim(routes, tp_index * rows_own, rows_own, 0)
    if (
        tp_count == 4 and sp_count % 2 == 0 and sp_count <= 16 and local_heads <= 8
        and rows_own <= 128 and rows_own < 2 * capacity
    ):
        return fused_layer(
            query_rows, key_rows, value_rows, gate_rows, log_decay, head_gain, out_weight, residual, ffn_gain,
            gate_weight[0], up_weight[0], down_weight[0], own_routes, route_weights,
        )
    hidden = retention(query_rows, key_rows, value_rows, gate_rows, log_decay, head_gain)
    mixed = jnp.dot(hidden, out_weight, preferred_element_type=jnp.float32).astype(jnp.bfloat16)
    mixed_sum = lax.psum_scatter(mixed, "tp", scatter_dimension=0, tiled=True).astype(jnp.float32)
    updated = residual.astype(jnp.float32) + mixed_sum
    ffn_in = square_norm(updated, ffn_gain)
    own_experts, own_ranks = slot_ranks(own_routes, sp_count)
    home_slot = own_experts * capacity + own_ranks
    gate_part = gate_weight[0]
    up_part = up_weight[0]
    down_part = down_weight[0]
    empty_row = jnp.zeros((1, model_width), jnp.bfloat16)
    source_row = (
        jnp.full((sp_count * capacity,), rows_own, jnp.int32)
        .at[home_slot]
        .set(jnp.arange(rows_own * TOPK, dtype=jnp.int32) // TOPK)
    )
    padded = jnp.concatenate([ffn_in, empty_row], axis=0)
    outgoing = padded[source_row].reshape(sp_count, capacity, model_width)
    arrived = lax.all_to_all(outgoing, "sp", split_axis=0, concat_axis=0, tiled=True)
    fanned = lax.all_gather(arrived[None], "tp", axis=0, tiled=True)
    activity = expert_rows(fanned.reshape(-1, model_width), gate_part, up_part)
    partial_out = jnp.dot(activity, down_part, preferred_element_type=jnp.float32).reshape(
        tp_count, sp_count, capacity, model_width
    )
    summed = (
        lax.psum_scatter(partial_out.astype(jnp.bfloat16), "tp", scatter_dimension=0, tiled=True)
        .astype(jnp.float32)
        .reshape(sp_count, capacity, model_width)
    )
    returned = lax.all_to_all(
        summed.astype(jnp.bfloat16), "sp", split_axis=0, concat_axis=0, tiled=True
    )
    picked = returned.reshape(sp_count * capacity, model_width)[home_slot].reshape(
        rows_own, TOPK, model_width
    )
    expert_sum = jnp.sum(route_weights[:, :, None] * picked.astype(jnp.float32), axis=1)
    return (updated + expert_sum).astype(jnp.bfloat16)


def solution(mesh):
    return jax.shard_map(
        body,
        mesh=mesh,
        in_specs=(
            P("sp", "tp"),
            P("sp", "tp"),
            P("sp", "tp"),
            P("sp", "tp"),
            P("sp", "tp"),
            P("tp"),
            P("tp", None),
            P(("sp", "tp"), None),
            P(),
            P("sp", None, "tp"),
            P("sp", None, "tp"),
            P("sp", "tp", None),
            P("sp", None),
            P(("sp", "tp"), None),
        ),
        out_specs=P(("sp", "tp"), None),
        check_vma=False,
    )
```

time: 155 us -> 116 us (0.75)
  Pallas kernels: 140 us -> 111 us
  local copies, waits for them, and re-layouts: 8.38 us -> 3.16 us
  other arithmetic: 4.08 us -> 0.82 us
  matrix products: 2.73 us -> 0 us
    pallas_call x5 -> x1, Pallas kernels: 140 us -> 111 us  [fused_layer(): pl.pallas_call(functools.partial(layer_kernel, planes), out_shape=jax.Sha...]
    slice x5 -> x0, local copies, waits for them, and re-layouts: 3.32 us -> none  [the longest x1 1.63 us: retention(): state[:, :HEAD_DIM, :].astype(jnp.bfloat16)]
    dot_general x1 -> x0, matrix products: 2.73 us -> none  [body(): jnp.dot(hidden, out_weight, preferred_element_type=jnp.float32)]
where the time goes in v2:
time: 116 us; the launch traced here: 115 us
  Pallas kernels  111 us (96%)
  local copies, waits for them, and re-layouts  3.16 us (3%)
    pallas_call x1, Pallas kernels, fused_layer(): pl.pallas_call(functools.partial(layer_kernel, planes), out_shape=jax.Sha...  111 us
    unnamed x3, local copies, waits for them, and re-layouts  2.36 us

profile of v2, /device:TPU:0, one launch (start us, length us, event | category | flops | bytes accessed | tf_op | source)
XLA Modules:
  0.0 114.8 jit_solution(4196989576439315844)
XLA Ops:
  0.0 0.0 copy-start
  0.0 0.7 copy-done
  0.7 0.1 dynamic-slice_bitcast_fusion
  0.8 0.8 select_reduce_fusion
  1.6 0.1 copy.17
  1.7 0.6 pad.4.shares
  2.3 110.8 %shard_map.154 = bf16[64,2048]{1,0:T(8,128)(2,1)} custom-call(bf16[256,512]{1,0:T(8,128)(2,1)} %q_ref.1, bf16[256,512]{1,0:T(8,128)(2,1)} %k_ref.1, bf16[256,512]{1,0:T(8,128)(2,1)} %v_ref.1, bf16[256,512]{1,0:T(8,128)(2,1)} %gate_ref.1, f32[4,256]{1,0:T(4,128)} %bitcast.13, f32[1,512]{1,0:T(1,128)} %bitcast.14, f32[2,256,128]{2,1,0:T(8,128)} %constant.17.clone.near_table, ...), custom_call_target="tpu_custom_call" | custom-call | tf_op jit(solution)/shard_map/pallas_call | solution.py:616
  113.1 1.7 %copy.19 = bf16[64,2048]{1,0:T(8,128)(2,1)} copy(bf16[64,2048]{1,0:T(8,128)(2,1)} %shard_map.154) | data formatting | bytes 524288
Async XLA Ops:
  0.0 0.7 copy-start

commit v3 on v2

--- a/solution.py
+++ b/solution.py
@@ -158,16 +158,17 @@
 
 (
     UP_A, UP_B, DOWN_A, DOWN_B, X_A2, Y_B2, Y_A3, Y_A4, X_B3, X_B4, C_A, C_B, C_P, Y_A, X_B, X_A, Y_B, RZ_A, RZ_B,
-    TOTAL, CHAIN, ACROSS, MIX_C, MIX_Y,
-) = range(24)
+    TOTAL, CHAIN, ACROSS, MIX_C, MIX_Y, S_X2, S_Y2, S_Y3, S_X3, S_Y4, S_X4, S_UP, S_DOWN, S_CORE,
+) = range(33)
 
 
 def layer_kernel(
-    planes, q_ref, k_ref, v_ref, gate_ref, logs, head_gain, near_table, base_table, residual, ffn_gain, shares,
+    planes, q_ref, k_ref, v_ref, gate_ref, logs, head_gain, near_table, base_table, residual, ffn_gain,
+    routes, route_weights,
     wo_hbm, wg_hbm, wu_hbm, wd_hbm, out,
     wo, wg, wu, wd, rotary, turned_k, ret, qdec, state, cum_col, cum_row, total_own, total_x, carry_in, carry_out,
     side_out, side_in, hidden, blend, from_core, held, from_y, upd,
-    g0, g1, pm, pr, a0, a1, r10, r11, b0, b1, r20, r21, d0, d1, z0, z1,
+    share_in, g0, g1, gs, pm, pr, a0, a1, r10, r11, b0, b1, r20, r21, d0, d1, z0, z1,
     ssem, rsem, wsem,
 ):
     sp, tp = lax.axis_index("sp"), lax.axis_index("tp")
@@ -176,6 +177,8 @@
     y, c = tp // 2, tp % 2
     own_rows, width = out.shape
     half = width // 2
+    wide_a, wide_b = g0.shape[-1] - 128, g1.shape[-1]
+    wide_ab = wide_a + wide_b
     rows = own_rows // 2
     items = 2 * planes
     lag = items - 3
@@ -371,15 +374,69 @@
     other_x = (1 - x) * 2 + y
     other_y = x * 2 + (1 - y)
     other_xy = (1 - x) * 2 + (1 - y)
-    share = jnp.transpose(shares[...])[:own_rows, :]
+    count = routes.shape[0]
+    share_in[...] = jnp.zeros_like(share_in)
+    share_in[:count, :own_rows] = route_weights[...]
+    all_routes = jnp.concatenate([routes[...]] * (8 // count), axis=0)
+    own_routes = jnp.zeros((8, 128), jnp.int32)
+    for q in range(4):
+        turned_routes = pltpu.roll(all_routes, (length - q * own_rows) % length, 1)
+        own_routes = own_routes + jnp.where(tp == q, turned_routes[:, :128], 0)
+    expert = lax.broadcasted_iota(jnp.int32, (128, 128), 0)
+    shares = jnp.zeros((128, 128), f32)
+    for k in range(count):
+        shares = shares + jnp.where(own_routes[k : k + 1, :] == expert, share_in[k : k + 1, :], 0.0)
+    share = jnp.transpose(shares)[:own_rows, :]
     coarse = share.astype(bf16).astype(f32)
     tail_rows = (coarse + pltpu.roll(share - coarse, sp_count, 1)).astype(bf16)
+    first_rows, last_rows = pl.ds(0, rows), pl.ds(rows, rows)
     for r in range(2):
         mine, n = slice(r * rows, (r + 1) * rows), 2 * z + r
         ready = (upd[mine, :] * scale[mine] * ffn_gain[...]).astype(bf16)
-        g0[c, n, here, :, :half] = ready[:, :half]
-        g0[c, n, here, :, half:] = tail_rows[mine]
-        g1[c, n, here] = ready[:, half:]
+        g0[c, n, here, :, :wide_a] = ready[:, :wide_a]
+        g0[c, n, here, :, wide_a:] = tail_rows[mine]
+        g1[c, n, here] = ready[:, wide_a:wide_ab]
+        gs[c, z, here, mine, :] = ready[:, wide_ab:]
+
+    def side(p, chip, part):
+        return gs.at[c, p, chip, part]
+
+    def pass_side(kind, n, chip, part, device):
+        send(kind, n, side(z, chip, part), side(z, chip, part), device)
+
+    def spread_side():
+        pass_side(S_X2, 0, here, first_rows, to_x)
+        pass_side(S_Y2, 0, here, last_rows, to_y)
+        pass_side(S_Y3, 0, here, first_rows, to_y)
+        pass_side(S_X3, 0, here, last_rows, to_x)
+
+    def relay_side():
+        arrived(S_X2, 0, side(z, other_x, first_rows))
+        pass_side(S_Y4, 0, other_x, first_rows, to_y)
+        arrived(S_Y2, 0, side(z, other_y, last_rows))
+        pass_side(S_X4, 0, other_y, last_rows, to_x)
+
+    def side_up(p):
+        @pl.when(z + 1 < planes)
+        def _():
+            send(S_UP, p, gs.at[c, p], gs.at[c, p], at_plane(z + 1))
+
+    def side_down(p):
+        @pl.when(z > 0)
+        def _():
+            send(S_DOWN, p, gs.at[c, p], gs.at[c, p], at_plane(z - 1))
+
+    def side_core(p):
+        send(S_CORE, p, gs.at[c, p], gs.at[c, p], to_core)
+
+    def close_side():
+        arrived(S_Y3, 0, side(z, other_y, first_rows))
+        arrived(S_Y4, 0, side(z, other_xy, first_rows))
+        arrived(S_X3, 0, side(z, other_x, last_rows))
+        arrived(S_X4, 0, side(z, other_xy, last_rows))
+        side_up(z)
+        side_down(z)
+        side_core(z)
 
     def spread(n):
         send(X_A2, n, g0.at[c, n, here], g0.at[c, n, here], to_x)
@@ -399,6 +456,7 @@
             send(DOWN_A, n, g0.at[c, n, here], g0.at[c, n, here], at_plane(z - 1))
             send(DOWN_B, n, g1.at[c, n, here], g1.at[c, n, here], at_plane(z - 1))
 
+    spread_side()
     spread(2 * z)
     for r in range(2):
         raise_up(2 * z + r)
@@ -412,7 +470,9 @@
             arrived(Y_B2, n, g1.at[c, n, other_y])
             send(X_B4, n, g1.at[c, n, other_y], g1.at[c, n, other_y], to_x)
 
+        pl.when(t == 0)(relay_side)
         pl.when(t == 0)(relay)
+        pl.when(t == 1)(close_side)
 
         @pl.when(t + 1 < items)
         def _():
@@ -436,6 +496,22 @@
 
         pl.when((t > 0) & (t < items))(relay)
 
+        @pl.when((t >= 2) & (t < items) & (t % 2 == 0))
+        def _():
+            below, above = z - t // 2, z + t // 2
+
+            @pl.when(below >= 0)
+            def _():
+                arrived(S_UP, below, gs.at[c, below])
+                side_up(below)
+                side_core(below)
+
+            @pl.when(above < planes)
+            def _():
+                arrived(S_DOWN, above, gs.at[c, above])
+                side_down(above)
+                side_core(above)
+
         @pl.when(t == 2)
         def _():
             for copy in weights[1:]:
@@ -446,19 +522,24 @@
             n = item_of(t - 2)
             arrived(C_A, n, g0.at[1 - c, n])
             arrived(C_B, n, g1.at[1 - c, n])
-            lead = g0[:, n].reshape(8 * rows, half + 128)
-            tail = lead[:, half:].astype(f32)
-            lead = lead[:, :half]
-            rest = g1[:, n].reshape(8 * rows, half)
+            p, r = plane_of(t - 2), half_of(t - 2)
+
+            @pl.when(r == 0)
+            def _():
+                arrived(S_CORE, p, gs.at[1 - c, p])
+
+            lead = g0[:, n].reshape(8 * rows, wide_a + 128)
+            tail = lead[:, wide_a:].astype(f32)
+            rest = g1[:, n].reshape(8 * rows, wide_b)
+            last = gs[:, p, :, pl.ds(pl.multiple_of(r * rows, rows), rows), :].reshape(8 * rows, width - wide_ab)
+            rows_in = jnp.concatenate([lead[:, :wide_a], rest, last], axis=1)
             lane = lax.broadcasted_iota(jnp.int32, tail.shape, 1)
             weight = jnp.sum(
                 jnp.where((lane == sp) | (lane == sp + sp_count), tail, 0.0), axis=1, keepdims=True
             )
 
             def product(w):
-                return jnp.dot(lead, w[:half, :], preferred_element_type=f32) + jnp.dot(
-                    rest, w[half:, :], preferred_element_type=f32
-                )
+                return jnp.dot(rows_in, w[...], preferred_element_type=f32)
 
             gate = jnp.minimum(product(wg), clamp_limit)
             up = jnp.clip(product(wu), -clamp_limit, clamp_limit)
@@ -564,6 +645,26 @@
         return carry
 
     lax.fori_loop(0, items, drain, 0)
+    left(S_X2, 0, side(z, here, first_rows))
+    left(S_Y2, 0, side(z, here, last_rows))
+    left(S_Y3, 0, side(z, here, first_rows))
+    left(S_X3, 0, side(z, here, last_rows))
+    left(S_Y4, 0, side(z, other_x, first_rows))
+    left(S_X4, 0, side(z, other_y, last_rows))
+
+    def drain_side(p, carry):
+        @pl.when((p <= z) & (z + 1 < planes))
+        def _():
+            left(S_UP, p, gs.at[c, p])
+
+        @pl.when((p >= z) & (z > 0))
+        def _():
+            left(S_DOWN, p, gs.at[c, p])
+
+        left(S_CORE, p, gs.at[c, p])
+        return carry
+
+    lax.fori_loop(0, planes, drain_side, 0)
     left(TOTAL, 0, total_own)
     for h in range(heads):
         left(ACROSS, h, side_out.at[h])
@@ -593,15 +694,12 @@
 
 def fused_layer(
     query_rows, key_rows, value_rows, gate_rows, log_decay, head_gain, out_weight, residual, ffn_gain,
-    gate_part, up_part, down_part, own_routes, route_weights,
+    gate_part, up_part, down_part, routes, route_weights,
 ):
     sp_count = lax.axis_size("sp")
     length, heads = log_decay.shape
     rows_all, width = residual.shape
     inner = query_rows.shape[1]
-    chosen = own_routes.T[:, None, :] == jnp.arange(128, dtype=jnp.int32)[None, :, None]
-    shares = jnp.sum(jnp.where(chosen, route_weights.T[:, None, :], 0.0), axis=0)
-    shares = jnp.pad(shares, ((0, 0), (0, 128 - rows_all)))
     near_table, base_table = rope_tables(length, sp_count)
     half = width // 2
     planes = sp_count // 2
@@ -609,6 +707,9 @@
     rows = rows_all // 2
     pieces = 4
     span = width // pieces
+    wide_s = 128 * (3 * width // 2048)
+    wide_a = (width - wide_s - 128) // 256 * 128
+    wide_b = width - wide_s - wide_a
     bf16, f32 = jnp.bfloat16, jnp.float32
     whole = pl.BlockSpec(memory_space=pltpu.VMEM)
     far = pl.BlockSpec(memory_space=pl.ANY)
@@ -616,7 +717,7 @@
     return pl.pallas_call(
         functools.partial(layer_kernel, planes),
         out_shape=jax.ShapeDtypeStruct((rows_all, width), bf16),
-        in_specs=[whole] * 11 + [far] * 4,
+        in_specs=[whole] * 12 + [far] * 4,
         out_specs=whole,
         scratch_shapes=[
             pltpu.VMEM(out_weight.shape, bf16),
@@ -642,8 +743,10 @@
             pltpu.VMEM((pieces, rows_all, span), bf16),
             pltpu.VMEM((pieces, rows_all, span), bf16),
             pltpu.VMEM((rows_all, width), f32),
-            pltpu.VMEM((2, items, 4, rows, half + 128), bf16),
-            pltpu.VMEM((2, items, 4, rows, half), bf16),
+            pltpu.VMEM((8, 128), f32),
+            pltpu.VMEM((2, items, 4, rows, wide_a + 128), bf16),
+            pltpu.VMEM((2, items, 4, rows, wide_b), bf16),
+            pltpu.VMEM((2, planes, 4, rows_all, wide_s), bf16),
             pltpu.VMEM((items, 2, 4 * rows, width), bf16),
             pltpu.VMEM((items, 4 * rows, width), bf16),
             pltpu.VMEM((items, 2, 2, rows, half), bf16),
@@ -658,8 +761,8 @@
             pltpu.VMEM((items, rows, half), bf16),
             pltpu.VMEM((items, rows, half), bf16),
             pltpu.VMEM((items, rows, half), bf16),
-            pltpu.SemaphoreType.DMA((24, max(items, heads))),
-            pltpu.SemaphoreType.DMA((24, max(items, heads))),
+            pltpu.SemaphoreType.DMA((33, max(items, heads))),
+            pltpu.SemaphoreType.DMA((33, max(items, heads))),
             pltpu.SemaphoreType.DMA((4,)),
         ],
         compiler_params=pltpu.CompilerParams(
@@ -667,7 +770,7 @@
         ),
     )(
         query_rows, key_rows, value_rows, gate_rows, log_decay.T, head_gain[None, :], near_table, base_table,
-        residual, ffn_gain[None, :], shares, out_weight, gate_part, up_part, down_part,
+        residual, ffn_gain[None, :], routes.T, route_weights.T, out_weight, gate_part, up_part, down_part,
     )
 
 
@@ -695,15 +798,15 @@
     rows_own = tok_count // tp_count
     capacity = max(2, 3 * rows_own * TOPK // (2 * sp_count))
     tp_index = lax.axis_index("tp")
-    own_routes = lax.dynamic_slice_in_dim(routes, tp_index * rows_own, rows_own, 0)
     if (
         tp_count == 4 and sp_count % 2 == 0 and sp_count <= 16 and local_heads <= 8
-        and rows_own <= 128 and rows_own < 2 * capacity
+        and rows_own <= 128 and rows_own < 2 * capacity and model_width % 2048 == 0
     ):
         return fused_layer(
             query_rows, key_rows, value_rows, gate_rows, log_decay, head_gain, out_weight, residual, ffn_gain,
-            gate_weight[0], up_weight[0], down_weight[0], own_routes, route_weights,
+            gate_weight[0], up_weight[0], down_weight[0], routes, route_weights,
         )
+    own_routes = lax.dynamic_slice_in_dim(routes, tp_index * rows_own, rows_own, 0)
     hidden = retention(query_rows, key_rows, value_rows, gate_rows, log_decay, head_gain)
     mixed = jnp.dot(hidden, out_weight, preferred_element_type=jnp.float32).astype(jnp.bfloat16)
     mixed_sum = lax.psum_scatter(mixed, "tp", scatter_dimension=0, tiled=True).astype(jnp.float32)

time: 116 us -> 114 us (0.983)
  local copies, waits for them, and re-layouts: 3.16 us -> 1.67 us
    pallas_call x1, Pallas kernels: 111 us -> 112 us  [fused_layer(): pl.pallas_call(functools.partial(layer_kernel, planes), out_shape=jax.Sha...]
    unnamed x3 -> x1, local copies, waits for them, and re-layouts: 2.36 us -> 1.67 us
where the time goes in v3:
time: 114 us
  Pallas kernels  112 us (98%)
  local copies, waits for them, and re-layouts  1.67 us (1%)
    pallas_call x1, Pallas kernels, fused_layer(): pl.pallas_call(functools.partial(layer_kernel, planes), out_shape=jax.Sha...  112 us

profile of v3, /device:TPU:0, one launch (start us, length us, event | category | flops | bytes accessed | tf_op | source)
XLA Modules:
  0.0 113.8 jit_solution(11525977137678935929)
XLA Ops:
  0.0 112.1 %shard_map.154 = bf16[64,2048]{1,0:T(8,128)(2,1)} custom-call(bf16[256,512]{1,0:T(8,128)(2,1)} %q_ref.1, bf16[256,512]{1,0:T(8,128)(2,1)} %k_ref.1, bf16[256,512]{1,0:T(8,128)(2,1)} %v_ref.1, bf16[256,512]{1,0:T(8,128)(2,1)} %gate_ref.1, f32[4,256]{1,0:T(4,128)} %bitcast.12, f32[1,512]{1,0:T(1,128)} %bitcast.14, f32[2,256,128]{2,1,0:T(8,128)} %constant.4.clone.near_table, ...), custom_call_target="tpu_custom_call" | custom-call | tf_op jit(solution)/shard_map/pallas_call | solution.py:717
  112.1 1.7 %copy.18 = bf16[64,2048]{1,0:T(8,128)(2,1)} copy(bf16[64,2048]{1,0:T(8,128)(2,1)} %shard_map.154) | data formatting | bytes 524288

commit v4 on v3

--- a/solution.py
+++ b/solution.py
@@ -163,10 +163,10 @@
 
 
 def layer_kernel(
-    planes, q_ref, k_ref, v_ref, gate_ref, logs, head_gain, near_table, base_table, residual, ffn_gain,
-    routes, route_weights,
-    wo_hbm, wg_hbm, wu_hbm, wd_hbm, out,
-    wo, wg, wu, wd, rotary, turned_k, ret, qdec, state, cum_col, cum_row, total_own, total_x, carry_in, carry_out,
+    planes, logs_hbm, k_hbm, near_hbm, base_hbm, v_hbm, q_hbm, gate_hbm, gain_hbm, routes_hbm, shares_hbm,
+    residual_hbm, ffn_gain_hbm, wo_hbm, wg_hbm, wu_hbm, wd_hbm, out,
+    logs, k_ref, near_table, base_table, v_ref, q_ref, gate_ref, head_gain, routes, route_weights,
+    residual, ffn_gain, wo, wg, wu, wd, rotary, turned_k, ret, qdec, state, cum_col, cum_row, total_own, total_x, carry_in, carry_out,
     side_out, side_in, hidden, blend, from_core, held, from_y, upd,
     share_in, g0, g1, gs, pm, pr, a0, a1, r10, r11, b0, b1, r20, r21, d0, d1, z0, z1,
     ssem, rsem, wsem,
@@ -203,14 +203,12 @@
         return 2 * plane_of(n) + half_of(n)
 
     def step_of(turn):
-        back = items - 3 - 2 * ((turn - 1) // 2) + (turn - 1) % 2
-        return jnp.where((turn == 0) | (turn == items - 1), turn, back)
-
-    def turn_at(u):
-        return jnp.where(u == 0, 0, u - 1)
+        back = items - 3 - 2 * ((turn - 2) // 2) + turn % 2
+        kept = (turn <= 1) | (turn == items - 1)
+        return jnp.where(kept, turn, jnp.where(turn == items - 2, 2, back))
 
     def has_turn(u):
-        return (u == 0) | ((u >= 2) & (u <= items))
+        return (u >= 0) & (u < items)
 
     def at_plane(p):
         return {"sp": p * 2 + x, "tp": tp}
@@ -234,26 +232,33 @@
     def left(kind, n, src):
         move(kind, n, src, src, to_core).wait_send()
 
+    loads = [
+        pltpu.make_async_copy(far, near, wsem.at[i])
+        for i, (far, near) in enumerate(
+            [
+                (logs_hbm, logs), (k_hbm, k_ref), (near_hbm, near_table), (base_hbm, base_table), (v_hbm, v_ref),
+                (q_hbm, q_ref), (gate_hbm, gate_ref), (gain_hbm, head_gain), (routes_hbm, routes),
+                (shares_hbm, route_weights), (residual_hbm, residual), (ffn_gain_hbm, ffn_gain),
+                (wo_hbm, wo), (wg_hbm, wg), (wu_hbm, wu), (wd_hbm, wd),
+            ]
+        )
+    ]
+    for copy in loads:
+        copy.start()
     barrier = pltpu.get_barrier_semaphore()
     for device in [to_core, to_y, to_x] + [to_z(i) for i in range(1, planes)]:
         pl.semaphore_signal(barrier, inc=1, device_id=device, device_id_type=pl.DeviceIdType.MESH)
 
-    weights = [
-        pltpu.make_async_copy(wo_hbm, wo, wsem.at[0]),
-        pltpu.make_async_copy(wg_hbm, wg, wsem.at[1]),
-        pltpu.make_async_copy(wu_hbm, wu, wsem.at[2]),
-        pltpu.make_async_copy(wd_hbm, wd, wsem.at[3]),
-    ]
-    for copy in weights:
-        copy.start()
-
     length = q_ref.shape[0]
-    heads = state.shape[0]
     dim = HEAD_DIM
+    heads = q_ref.shape[1] // dim
+    depth = state.shape[1]
+    cuts = dim // depth
     after = lax.broadcasted_iota(jnp.int32, (length, length), 0) >= lax.broadcasted_iota(
         jnp.int32, (length, length), 1
     )
     ones = jnp.where(after, 1.0, 0.0).astype(f32)
+    loads[0].wait()
     log_rows = jnp.concatenate([logs[...], jnp.zeros((8 - heads, length), f32)], axis=0)
     cum_row[...] = lax.dot_general(
         log_rows, ones, (((1,), (1,)), ((), ())), precision=highest, preferred_element_type=f32
@@ -265,6 +270,8 @@
     pl.semaphore_wait(barrier, 2 + planes)
     send(TOTAL, 0, total_own, total_x, to_x)
 
+    loads[2].wait()
+    loads[3].wait()
     base = base_table[pl.ds(sp * 8, 8), :]
     cosine = base[0:1] * near_table[0] - base[1:2] * near_table[1]
     sine = base[2:3] * near_table[0] + base[3:4] * near_table[1]
@@ -279,15 +286,44 @@
         lanes = lax.broadcasted_iota(jnp.int32, cum_col.shape, 1)
         return jnp.sum(jnp.where(lanes == h, cum_col[...], 0.0), axis=1, keepdims=True)
 
+    left_side = x == 0
+
+    def pass_state(e):
+        h = e // cuts
+        own_total, x_total = total_own[h : h + 1, :], total_x[h : h + 1, :]
+        before = carry_in[e].astype(f32)
+
+        @pl.when(z + 1 < planes)
+        def _():
+            fresh = jnp.where(left_side, jnp.exp(x_total), 1.0) * state[e]
+            carry_out[e] = (jnp.exp(own_total + x_total) * before + fresh).astype(bf16)
+            send(CHAIN, e, carry_out.at[e], carry_in.at[e], at_plane(z + 1))
+
+        side_out[e] = jnp.where(left_side, jnp.exp(own_total) * before + state[e], before).astype(bf16)
+        send(ACROSS, e, side_out.at[e], side_in.at[e], to_x)
+
+    @pl.when(z == 0)
+    def _():
+        carry_in[...] = jnp.zeros_like(carry_in)
+
+    loads[1].wait()
+    loads[4].wait()
     for h in range(heads):
         lanes = pl.ds(h * dim, dim)
         keys = turned(k_ref[:, lanes]) * dim ** (-0.5)
         turned_k[:, lanes] = keys.astype(bf16)
         column = column_of(h)
         tailed = (keys * jnp.exp(column[length - 1 :, :] - column)).astype(bf16)
-        state[h] = lax.dot_general(
+        state[cuts * h : cuts * (h + 1)] = lax.dot_general(
             tailed, v_ref[:, lanes], (((0,), (0,)), ((), ())), preferred_element_type=f32
-        )
+        ).reshape(cuts, depth, dim)
+
+        @pl.when(z == 0)
+        def _():
+            if h == 0:
+                arrived(TOTAL, 0, total_x)
+            for e in range(cuts * h, cuts * (h + 1)):
+                pass_state(e)
 
     def attend(h, carry):
         lanes = pl.ds(pl.multiple_of(h * dim, dim), dim)
@@ -303,49 +339,45 @@
         return carry
 
     early = jnp.where(z >= planes // 2, heads, 0)
+    loads[5].wait()
     lax.fori_loop(0, early, attend, 0)
 
-    arrived(TOTAL, 0, total_x)
-    left_side = x == 0
-    for h in range(heads):
-        own_total, x_total = total_own[h : h + 1, :], total_x[h : h + 1, :]
+    @pl.when(z > 0)
+    def _():
+        arrived(TOTAL, 0, total_x)
+
+    for e in range(cuts * heads):
 
         @pl.when(z > 0)
         def _():
-            arrived(CHAIN, h, carry_in.at[h])
-
-        @pl.when(z == 0)
-        def _():
-            carry_in[h] = jnp.zeros((dim, dim), bf16)
-
-        before = carry_in[h].astype(f32)
-
-        @pl.when(z + 1 < planes)
-        def _():
-            fresh = jnp.where(left_side, jnp.exp(x_total), 1.0) * state[h]
-            carry_out[h] = (jnp.exp(own_total + x_total) * before + fresh).astype(bf16)
-            send(CHAIN, h, carry_out.at[h], carry_in.at[h], at_plane(z + 1))
-
-        side_out[h] = jnp.where(left_side, jnp.exp(own_total) * before + state[h], before).astype(bf16)
-        send(ACROSS, h, side_out.at[h], side_in.at[h], to_x)
+            arrived(CHAIN, e, carry_in.at[e])
+            pass_state(e)
 
     lax.fori_loop(early, heads, attend, 0)
 
     for h in range(heads):
         lanes = pl.ds(h * dim, dim)
-        arrived(ACROSS, h, side_in.at[h])
+        if h == 0:
+            loads[6].wait()
+            loads[7].wait()
+        blocks = slice(cuts * h, cuts * (h + 1))
+        for e in range(cuts * h, cuts * (h + 1)):
+            arrived(ACROSS, e, side_in.at[e])
         factor = jnp.where(left_side, 1.0, jnp.exp(total_x[h : h + 1, :]))
-        entering = (factor * carry_in[h].astype(f32) + side_in[h].astype(f32)).astype(bf16)
+        before = carry_in[blocks].reshape(dim, dim).astype(f32)
+        entering = (factor * before + side_in[blocks].reshape(dim, dim).astype(f32)).astype(bf16)
         retained = ret[:, lanes] + jnp.dot(qdec[:, lanes], entering, preferred_element_type=f32)
         centred = retained - jnp.mean(retained, axis=-1, keepdims=True)
         variance = jnp.mean(centred * centred, axis=-1, keepdims=True)
         gate_in = gate_ref[:, lanes].astype(f32)
         scaled = centred * lax.rsqrt(variance + group_eps) * head_gain[:, lanes]
-        hidden[:, lanes] = (scaled * (gate_in / (1.0 + jnp.exp(-gate_in)))).astype(bf16)
-
-    weights[0].wait()
+        made = (scaled * (gate_in / (1.0 + jnp.exp(-gate_in)))).astype(bf16)
+        hidden[:, :, lanes] = made.reshape(4, own_rows, dim)
+
+    loads[12].wait()
     pieces = blend.shape[0]
-    span = width // pieces
+    spans = pieces // 2
+    span = width // spans
 
     def cross(j):
         arrived(MIX_C, j, from_core.at[j])
@@ -353,27 +385,21 @@
         send(MIX_Y, j, held.at[j], from_y.at[j], to_y)
 
     for j in range(pieces):
-        mixed = jnp.dot(hidden[...], wo[:, pl.ds(j * span, span)], preferred_element_type=f32).astype(bf16)
+        picked = hidden[:, j // spans * rows : (j // spans + 1) * rows, :].reshape(4 * rows, heads * dim)
+        mixed = jnp.dot(picked, wo[:, pl.ds(j % spans * span, span)], preferred_element_type=f32).astype(bf16)
         for q in range(4):
-            blend[j, q % 2, q // 2] = mixed[q * own_rows : (q + 1) * own_rows, :]
+            blend[j, q % 2, q // 2] = mixed[q * rows : (q + 1) * rows, :]
         send(MIX_C, j, blend.at[j, 1 - c], from_core.at[j], to_core)
         if j > 0:
             cross(j - 1)
     cross(pieces - 1)
-    square = jnp.zeros((own_rows, 1), f32)
-    for j in range(pieces):
-        cols = pl.ds(j * span, span)
-        base_rows = residual[:, cols].astype(f32) + blend[j, c, y].astype(f32) + from_core[j, y].astype(f32)
-        arrived(MIX_Y, j, from_y.at[j])
-        total = base_rows + from_y[j].astype(f32)
-        upd[:, cols] = total
-        square = square + jnp.sum(total * total, axis=-1, keepdims=True)
-    scale = lax.rsqrt(square * (1.0 / width) + square_eps)
 
     here = x * 2 + y
     other_x = (1 - x) * 2 + y
     other_y = x * 2 + (1 - y)
     other_xy = (1 - x) * 2 + (1 - y)
+    for copy in loads[8:12]:
+        copy.wait()
     count = routes.shape[0]
     share_in[...] = jnp.zeros_like(share_in)
     share_in[:count, :own_rows] = route_weights[...]
@@ -390,25 +416,19 @@
     coarse = share.astype(bf16).astype(f32)
     tail_rows = (coarse + pltpu.roll(share - coarse, sp_count, 1)).astype(bf16)
     first_rows, last_rows = pl.ds(0, rows), pl.ds(rows, rows)
-    for r in range(2):
-        mine, n = slice(r * rows, (r + 1) * rows), 2 * z + r
-        ready = (upd[mine, :] * scale[mine] * ffn_gain[...]).astype(bf16)
-        g0[c, n, here, :, :wide_a] = ready[:, :wide_a]
-        g0[c, n, here, :, wide_a:] = tail_rows[mine]
-        g1[c, n, here] = ready[:, wide_a:wide_ab]
-        gs[c, z, here, mine, :] = ready[:, wide_ab:]
-
     def side(p, chip, part):
         return gs.at[c, p, chip, part]
 
     def pass_side(kind, n, chip, part, device):
         send(kind, n, side(z, chip, part), side(z, chip, part), device)
 
-    def spread_side():
-        pass_side(S_X2, 0, here, first_rows, to_x)
-        pass_side(S_Y2, 0, here, last_rows, to_y)
-        pass_side(S_Y3, 0, here, first_rows, to_y)
-        pass_side(S_X3, 0, here, last_rows, to_x)
+    def spread_side(r):
+        if r == 0:
+            pass_side(S_X2, 0, here, first_rows, to_x)
+            pass_side(S_Y3, 0, here, first_rows, to_y)
+        else:
+            pass_side(S_Y2, 0, here, last_rows, to_y)
+            pass_side(S_X3, 0, here, last_rows, to_x)
 
     def relay_side():
         arrived(S_X2, 0, side(z, other_x, first_rows))
@@ -456,11 +476,27 @@
             send(DOWN_A, n, g0.at[c, n, here], g0.at[c, n, here], at_plane(z - 1))
             send(DOWN_B, n, g1.at[c, n, here], g1.at[c, n, here], at_plane(z - 1))
 
-    spread_side()
-    spread(2 * z)
     for r in range(2):
-        raise_up(2 * z + r)
-        hand_down(2 * z + r)
+        mine, n = slice(r * rows, (r + 1) * rows), 2 * z + r
+        square = jnp.zeros((rows, 1), f32)
+        for j in range(r * spans, (r + 1) * spans):
+            cols = pl.ds(j % spans * span, span)
+            near = residual[mine, cols].astype(f32) + blend[j, c, y].astype(f32) + from_core[j, y].astype(f32)
+            arrived(MIX_Y, j, from_y.at[j])
+            total = near + from_y[j].astype(f32)
+            upd[mine, cols] = total
+            square = square + jnp.sum(total * total, axis=-1, keepdims=True)
+        scale = lax.rsqrt(square * (1.0 / width) + square_eps)
+        ready = (upd[mine, :] * scale * ffn_gain[...]).astype(bf16)
+        g0[c, n, here, :, :wide_a] = ready[:, :wide_a]
+        g0[c, n, here, :, wide_a:] = tail_rows[mine]
+        g1[c, n, here] = ready[:, wide_a:wide_ab]
+        gs[c, z, here, mine, :] = ready[:, wide_ab:]
+        raise_up(n)
+        hand_down(n)
+        spread_side(r)
+        if r == 0:
+            spread(n)
 
     def tick(t, carry):
         def relay():
@@ -514,7 +550,7 @@
 
         @pl.when(t == 2)
         def _():
-            for copy in weights[1:]:
+            for copy in loads[13:]:
                 copy.wait()
 
         @pl.when((t >= 2) & (t < items + 2))
@@ -560,7 +596,7 @@
 
         @pl.when(has_turn(t - lag))
         def _():
-            n = item_of(step_of(turn_at(t - lag)))
+            n = item_of(step_of(t - lag))
             arrived(C_P, n, pr.at[n])
             for q in range(4):
                 part = pl.ds(q * rows, rows)
@@ -572,7 +608,7 @@
 
         @pl.when(has_turn(t - lag - 1))
         def _():
-            n = item_of(step_of(turn_at(t - lag - 1)))
+            n = item_of(step_of(t - lag - 1))
             arrived(Y_A, n, r10.at[n])
             b0[n] = (a0[n, y].astype(f32) + r10[n].astype(f32)).astype(bf16)
             send(X_A, n, b0.at[n, 1 - x], r20.at[n], to_x)
@@ -582,7 +618,7 @@
 
         @pl.when(has_turn(t - lag - 2))
         def _():
-            turn = step_of(turn_at(t - lag - 2))
+            turn = step_of(t - lag - 2)
             n = item_of(turn)
             arrived(X_A, n, r20.at[n])
             d0[n] = (b0[n, x].astype(f32) + r20[n].astype(f32)).astype(bf16)
@@ -597,7 +633,7 @@
 
         return carry
 
-    lax.fori_loop(0, items + lag + 3, tick, 0)
+    lax.fori_loop(0, items + lag + 2, tick, 0)
     for r in range(2):
         n, part = 2 * z + r, pl.ds(r * rows, rows)
         low = upd[part, :half] + d0[n].astype(f32)
@@ -666,12 +702,12 @@
 
     lax.fori_loop(0, planes, drain_side, 0)
     left(TOTAL, 0, total_own)
-    for h in range(heads):
-        left(ACROSS, h, side_out.at[h])
+    for e in range(cuts * heads):
+        left(ACROSS, e, side_out.at[e])
 
         @pl.when(z + 1 < planes)
         def _():
-            left(CHAIN, h, carry_out.at[h])
+            left(CHAIN, e, carry_out.at[e])
 
     for j in range(pieces):
         left(MIX_C, j, blend.at[j, 1 - c])
@@ -705,25 +741,26 @@
     planes = sp_count // 2
     items = 2 * planes
     rows = rows_all // 2
-    pieces = 4
-    span = width // pieces
+    pieces = 8
+    span = 2 * width // pieces
     wide_s = 128 * (3 * width // 2048)
     wide_a = (width - wide_s - 128) // 256 * 128
     wide_b = width - wide_s - wide_a
     bf16, f32 = jnp.bfloat16, jnp.float32
     whole = pl.BlockSpec(memory_space=pltpu.VMEM)
-    far = pl.BlockSpec(memory_space=pl.ANY)
-    square = (heads, HEAD_DIM, HEAD_DIM)
+    far = pl.BlockSpec(memory_space=pltpu.HBM)
+    operands = (
+        log_decay.T, key_rows, near_table, base_table, value_rows, query_rows, gate_rows, head_gain[None, :],
+        routes.T, route_weights.T, residual, ffn_gain[None, :], out_weight, gate_part, up_part, down_part,
+    )
+    square = (2 * heads, HEAD_DIM // 2, HEAD_DIM)
     return pl.pallas_call(
         functools.partial(layer_kernel, planes),
         out_shape=jax.ShapeDtypeStruct((rows_all, width), bf16),
-        in_specs=[whole] * 12 + [far] * 4,
+        in_specs=[far] * len(operands),
         out_specs=whole,
         scratch_shapes=[
-            pltpu.VMEM(out_weight.shape, bf16),
-            pltpu.VMEM(gate_part.shape, bf16),
-            pltpu.VMEM(up_part.shape, bf16),
-            pltpu.VMEM(down_part.shape, bf16),
+            *[pltpu.VMEM(operand.shape, operand.dtype) for operand in operands],
             pltpu.VMEM((2, length, HEAD_DIM), f32),
             pltpu.VMEM((length, inner), bf16),
             pltpu.VMEM((length, inner), f32),
@@ -737,11 +774,11 @@
             pltpu.VMEM(square, bf16),
             pltpu.VMEM(square, bf16),
             pltpu.VMEM(square, bf16),
-            pltpu.VMEM((length, inner), bf16),
-            pltpu.VMEM((pieces, 2, 2, rows_all, span), bf16),
-            pltpu.VMEM((pieces, 2, rows_all, span), bf16),
-            pltpu.VMEM((pieces, rows_all, span), bf16),
-            pltpu.VMEM((pieces, rows_all, span), bf16),
+            pltpu.VMEM((4, rows_all, inner), bf16),
+            pltpu.VMEM((pieces, 2, 2, rows, span), bf16),
+            pltpu.VMEM((pieces, 2, rows, span), bf16),
+            pltpu.VMEM((pieces, rows, span), bf16),
+            pltpu.VMEM((pieces, rows, span), bf16),
             pltpu.VMEM((rows_all, width), f32),
             pltpu.VMEM((8, 128), f32),
             pltpu.VMEM((2, items, 4, rows, wide_a + 128), bf16),
@@ -761,17 +798,14 @@
             pltpu.VMEM((items, rows, half), bf16),
             pltpu.VMEM((items, rows, half), bf16),
             pltpu.VMEM((items, rows, half), bf16),
-            pltpu.SemaphoreType.DMA((33, max(items, heads))),
-            pltpu.SemaphoreType.DMA((33, max(items, heads))),
-            pltpu.SemaphoreType.DMA((4,)),
+            pltpu.SemaphoreType.DMA((33, max(items, 2 * heads, pieces))),
+            pltpu.SemaphoreType.DMA((33, max(items, 2 * heads, pieces))),
+            pltpu.SemaphoreType.DMA((len(operands),)),
         ],
         compiler_params=pltpu.CompilerParams(
             collective_id=0, has_side_effects=True, vmem_limit_bytes=63 * 1024 * 1024
         ),
-    )(
-        query_rows, key_rows, value_rows, gate_rows, log_decay.T, head_gain[None, :], near_table, base_table,
-        residual, ffn_gain[None, :], routes.T, route_weights.T, out_weight, gate_part, up_part, down_part,
-    )
+    )(*operands)
 
 
 def body(

time: 114 us -> 107 us (0.939)
  the two profiles are of different devices: /device:TPU:0 before, /device:TPU:8 now
where the time goes in v4:
time: 107 us
  Pallas kernels  106 us (99%)
  local copies, waits for them, and re-layouts  1.67 us (2%)
    pallas_call x1, Pallas kernels, fused_layer(): pl.pallas_call(functools.partial(layer_kernel, planes), out_shape=jax.Sha...  106 us

profile of v4, /device:TPU:8, one launch (start us, length us, event | category | flops | bytes accessed | tf_op | source)
XLA Modules:
  0.0 107.2 jit_solution(13025952048156138411)
XLA Ops:
  0.0 105.5 %shard_map.154 = bf16[64,2048]{1,0:T(8,128)(2,1)} custom-call(f32[4,256]{1,0:T(4,128)} %bitcast.12, bf16[256,512]{1,0:T(8,128)(2,1)} %k_hbm.1, f32[2,256,128]{2,1,0:T(8,128)} %constant.4.clone.near_hbm, f32[64,128]{1,0:T(8,128)} %constant.5.clone.base_hbm, bf16[256,512]{1,0:T(8,128)(2,1)} %v_hbm.1, bf16[256,512]{1,0:T(8,128)(2,1)} %q_hbm.1, ...), custom_call_target="tpu_custom_call" | custom-call | tf_op jit(solution)/shard_map/pallas_call | solution.py:757
  105.5 1.7 %copy.18 = bf16[64,2048]{1,0:T(8,128)(2,1)} copy(bf16[64,2048]{1,0:T(8,128)(2,1)} %shard_map.154) | data formatting | bytes 524288

commit v5 on v4

--- a/solution.py
+++ b/solution.py
@@ -157,9 +157,10 @@
 
 
 (
-    UP_A, UP_B, DOWN_A, DOWN_B, X_A2, Y_B2, Y_A3, Y_A4, X_B3, X_B4, C_A, C_B, C_P, Y_A, X_B, X_A, Y_B, RZ_A, RZ_B,
+    UP_A, UP_B, DOWN_A, DOWN_B, X_A2, Y_B2, Y_A3, Y_A4, X_B3, X_B4, C_A, C_B, C_P, Y_A, X_B, X_A, Y_B, R_UP_A, R_UP_B,
     TOTAL, CHAIN, ACROSS, MIX_C, MIX_Y, S_X2, S_Y2, S_Y3, S_X3, S_Y4, S_X4, S_UP, S_DOWN, S_CORE,
-) = range(33)
+    T_UP, T_DOWN, T_Y1, T_X1, T_X2, T_Y2, R_DOWN_A, R_DOWN_B,
+) = range(41)
 
 
 def layer_kernel(
@@ -168,7 +169,8 @@
     logs, k_ref, near_table, base_table, v_ref, q_ref, gate_ref, head_gain, routes, route_weights,
     residual, ffn_gain, wo, wg, wu, wd, rotary, turned_k, ret, qdec, state, cum_col, cum_row, total_own, total_x, carry_in, carry_out,
     side_out, side_in, hidden, blend, from_core, held, from_y, upd,
-    share_in, g0, g1, gs, pm, pr, a0, a1, r10, r11, b0, b1, r20, r21, d0, d1, z0, z1,
+    share_in, g0, g1, gs, pm, pr, a0, a1, r10, r11, b0, b1, r20, r21, d0, d1, low_up, low_down, high_up, high_down,
+    tot, tot_up, tot_down, home, home_in, pair, pair_in,
     ssem, rsem, wsem,
 ):
     sp, tp = lax.axis_index("sp"), lax.axis_index("tp")
@@ -176,7 +178,7 @@
     z, x = sp // 2, sp % 2
     y, c = tp // 2, tp % 2
     own_rows, width = out.shape
-    half = width // 2
+    half = a0.shape[-1]
     wide_a, wide_b = g0.shape[-1] - 128, g1.shape[-1]
     wide_ab = wide_a + wide_b
     rows = own_rows // 2
@@ -305,6 +307,15 @@
     @pl.when(z == 0)
     def _():
         carry_in[...] = jnp.zeros_like(carry_in)
+        for r in range(2):
+            for ref in (tot_up, low_up, high_up):
+                ref[r] = jnp.zeros_like(ref[r])
+
+    @pl.when(z == planes - 1)
+    def _():
+        for r in range(2):
+            for ref in (tot_down, low_down, high_down):
+                ref[2 * planes - 2 + r] = jnp.zeros_like(ref[r])
 
     loads[1].wait()
     loads[4].wait()
@@ -498,6 +509,37 @@
         if r == 0:
             spread(n)
 
+    last_chains = [(T_UP, T_DOWN, tot, tot_up, tot_down)]
+    main_chains = [(R_UP_A, R_DOWN_A, d0, low_up, low_down), (R_UP_B, R_DOWN_B, d1, high_up, high_down)]
+
+    def start_chain(n, chains):
+        @pl.when((n // 2 > z) & (z == 0))
+        def _():
+            for up, _, acc, got_up, _ in chains:
+                send(up, n, acc.at[n], got_up.at[n], at_plane(z + 1))
+
+        @pl.when((n // 2 < z) & (z == planes - 1))
+        def _():
+            for _, down, acc, _, got_down in chains:
+                send(down, n, acc.at[n], got_down.at[n], at_plane(z - 1))
+
+    def go_on(turn, chains):
+        n = item_of(step_of(turn))
+
+        @pl.when((n // 2 > z) & (z > 0))
+        def _():
+            for up, _, acc, got_up, _ in chains:
+                arrived(up, n, got_up.at[n])
+                acc[n] = (acc[n].astype(f32) + got_up[n].astype(f32)).astype(bf16)
+                send(up, n, acc.at[n], got_up.at[n], at_plane(z + 1))
+
+        @pl.when((n // 2 < z) & (z < planes - 1))
+        def _():
+            for _, down, acc, _, got_down in chains:
+                arrived(down, n, got_down.at[n])
+                acc[n] = (acc[n].astype(f32) + got_down[n].astype(f32)).astype(bf16)
+                send(down, n, acc.at[n], got_down.at[n], at_plane(z - 1))
+
     def tick(t, carry):
         def relay():
             n = item_of(t)
@@ -581,7 +623,7 @@
             up = jnp.clip(product(wu), -clamp_limit, clamp_limit)
             act = ((up + 1.0) * (gate / (1.0 + jnp.exp(-swish_alpha * gate)))).astype(bf16)
             made = (jnp.dot(act, wd[...], preferred_element_type=f32) * weight).astype(bf16)
-            pm[n] = made.reshape(2, 4 * rows, 2 * half)
+            pm[n] = made.reshape(2, 4 * rows, width)
             send(C_P, n, pm.at[n, 1 - c], pr.at[n], to_core)
 
         @pl.when((t >= 1) & (t < items + 1))
@@ -602,9 +644,11 @@
                 part = pl.ds(q * rows, rows)
                 total = (pm[n, c, part, :].astype(f32) + pr[n, part, :].astype(f32)).astype(bf16)
                 a0[n, q % 2, q // 2] = total[:, :half]
-                a1[n, q // 2, q % 2] = total[:, half:]
+                a1[n, q // 2, q % 2] = total[:, half : 2 * half]
+                tot[n, q] = total[:, 2 * half :]
             send(Y_A, n, a0.at[n, 1 - y], r10.at[n], to_y)
             send(X_B, n, a1.at[n, 1 - x], r11.at[n], to_x)
+            start_chain(n, last_chains)
 
         @pl.when(has_turn(t - lag - 1))
         def _():
@@ -618,38 +662,109 @@
 
         @pl.when(has_turn(t - lag - 2))
         def _():
-            turn = step_of(t - lag - 2)
-            n = item_of(turn)
+            n = item_of(step_of(t - lag - 2))
             arrived(X_A, n, r20.at[n])
             d0[n] = (b0[n, x].astype(f32) + r20[n].astype(f32)).astype(bf16)
             arrived(Y_B, n, r21.at[n])
             d1[n] = (b1[n, y].astype(f32) + r21[n].astype(f32)).astype(bf16)
-
-            @pl.when((turn > 0) & (turn < items - 1))
-            def _():
-                m = 2 * z + half_of(turn)
-                send(RZ_A, n, d0.at[n], z0.at[m], at_plane(plane_of(turn)), m)
-                send(RZ_B, n, d1.at[n], z1.at[m], at_plane(plane_of(turn)), m)
+            start_chain(n, main_chains)
+
+        u = t - lag
+
+        @pl.when((u >= 3) & (u <= items - 2))
+        def _():
+            go_on(u - 1, last_chains)
+
+        @pl.when(u == items - 2)
+        def _():
+            go_on(1, last_chains)
+            go_on(items - 2, last_chains)
+
+        @pl.when((u >= 5) & (u <= items))
+        def _():
+            go_on(u - 3, main_chains)
+
+        @pl.when(u == items)
+        def _():
+            go_on(1, main_chains)
+            go_on(items - 2, main_chains)
+
+        @pl.when(u == items - 1)
+        def _():
+            for r in range(2):
+                n = 2 * z + r
+
+                @pl.when(z > 0)
+                def _():
+                    arrived(T_UP, n, tot_up.at[n])
+
+                @pl.when(z < planes - 1)
+                def _():
+                    arrived(T_DOWN, n, tot_down.at[n])
+
+                for q in range(4):
+                    total = tot[n, q].astype(f32) + tot_up[n, q].astype(f32) + tot_down[n, q].astype(f32)
+                    place = (q % 2, q // 2) if r == 0 else (q // 2, q % 2)
+                    home[r, place[0], place[1]] = total.astype(bf16)
+            send(T_Y1, 0, home.at[0, 1 - y], home_in.at[0], to_y)
+            send(T_X1, 0, home.at[1, 1 - x], home_in.at[1], to_x)
+
+        @pl.when(u == items)
+        def _():
+            arrived(T_Y1, 0, home_in.at[0])
+            pair[0] = (home[0, y].astype(f32) + home_in[0].astype(f32)).astype(bf16)
+            send(T_X2, 0, pair.at[0, 1 - x], pair_in.at[0], to_x)
+            arrived(T_X1, 0, home_in.at[1])
+            pair[1] = (home[1, x].astype(f32) + home_in[1].astype(f32)).astype(bf16)
+            send(T_Y2, 0, pair.at[1, 1 - y], pair_in.at[1], to_y)
 
         return carry
 
     lax.fori_loop(0, items + lag + 2, tick, 0)
+    arrived(T_X2, 0, pair_in.at[0])
+    arrived(T_Y2, 0, pair_in.at[1])
     for r in range(2):
         n, part = 2 * z + r, pl.ds(r * rows, rows)
         low = upd[part, :half] + d0[n].astype(f32)
-        high = upd[part, half:] + d1[n].astype(f32)
-        for i in range(1, planes):
-            n = 2 * ((z + i) % planes) + r
-            arrived(RZ_A, n, z0.at[n])
-            low = low + z0[n].astype(f32)
-            arrived(RZ_B, n, z1.at[n])
-            high = high + z1[n].astype(f32)
+        high = upd[part, half : 2 * half] + d1[n].astype(f32)
+
+        @pl.when(z > 0)
+        def _():
+            arrived(R_UP_A, n, low_up.at[n])
+            arrived(R_UP_B, n, high_up.at[n])
+
+        @pl.when(z < planes - 1)
+        def _():
+            arrived(R_DOWN_A, n, low_down.at[n])
+            arrived(R_DOWN_B, n, high_down.at[n])
+
+        low = low + low_up[n].astype(f32) + low_down[n].astype(f32)
+        high = high + high_up[n].astype(f32) + high_down[n].astype(f32)
         out[part, :half] = low.astype(bf16)
-        out[part, half:] = high.astype(bf16)
+        out[part, half : 2 * half] = high.astype(bf16)
+        kept = pair[0, x] if r == 0 else pair[1, y]
+        out[part, 2 * half :] = (
+            upd[part, 2 * half :] + kept.astype(f32) + pair_in[r].astype(f32)
+        ).astype(bf16)
+
+    left(T_Y1, 0, home.at[0, 1 - y])
+    left(T_X1, 0, home.at[1, 1 - x])
+    left(T_X2, 0, pair.at[0, 1 - x])
+    left(T_Y2, 0, pair.at[1, 1 - y])
 
     def drain(n, carry):
         p = n // 2
 
+        @pl.when(p > z)
+        def _():
+            for up, _, acc, _, _ in last_chains + main_chains:
+                left(up, n, acc.at[n])
+
+        @pl.when(p < z)
+        def _():
+            for _, down, acc, _, _ in last_chains + main_chains:
+                left(down, n, acc.at[n])
+
         @pl.when((p <= z) & (z + 1 < planes))
         def _():
             left(UP_A, n, g0.at[c, n, here])
@@ -659,11 +774,6 @@
         def _():
             left(DOWN_A, n, g0.at[c, n, here])
             left(DOWN_B, n, g1.at[c, n, here])
-
-        @pl.when((p < z) | (p > z))
-        def _():
-            left(RZ_A, n, d0.at[n])
-            left(RZ_B, n, d1.at[n])
 
         left(X_A2, n, g0.at[c, n, here])
         left(Y_B2, n, g1.at[c, n, here])
@@ -737,7 +847,8 @@
     rows_all, width = residual.shape
     inner = query_rows.shape[1]
     near_table, base_table = rope_tables(length, sp_count)
-    half = width // 2
+    wide_t = 128 * (width // 1024)
+    half = (width - wide_t) // 2
     planes = sp_count // 2
     items = 2 * planes
     rows = rows_all // 2
@@ -798,8 +909,17 @@
             pltpu.VMEM((items, rows, half), bf16),
             pltpu.VMEM((items, rows, half), bf16),
             pltpu.VMEM((items, rows, half), bf16),
-            pltpu.SemaphoreType.DMA((33, max(items, 2 * heads, pieces))),
-            pltpu.SemaphoreType.DMA((33, max(items, 2 * heads, pieces))),
+            pltpu.VMEM((items, rows, half), bf16),
+            pltpu.VMEM((items, rows, half), bf16),
+            pltpu.VMEM((items, 4, rows, wide_t), bf16),
+            pltpu.VMEM((items, 4, rows, wide_t), bf16),
+            pltpu.VMEM((items, 4, rows, wide_t), bf16),
+            pltpu.VMEM((2, 2, 2, rows, wide_t), bf16),
+            pltpu.VMEM((2, 2, rows, wide_t), bf16),
+            pltpu.VMEM((2, 2, rows, wide_t), bf16),
+            pltpu.VMEM((2, rows, wide_t), bf16),
+            pltpu.SemaphoreType.DMA((41, max(items, 2 * heads, pieces))),
+            pltpu.SemaphoreType.DMA((41, max(items, 2 * heads, pieces))),
             pltpu.SemaphoreType.DMA((len(operands),)),
         ],
         compiler_params=pltpu.CompilerParams(

time: 107 us -> 106 us (level)
  the two profiles are of different devices: /device:TPU:8 before, /device:TPU:0 now
where the time goes in v5:
time: 106 us
  Pallas kernels  104 us (98%)
  local copies, waits for them, and re-layouts  1.67 us (2%)
    pallas_call x1, Pallas kernels, fused_layer(): pl.pallas_call(functools.partial(layer_kernel, planes), out_shape=jax.Sha...  104 us

profile of v5, /device:TPU:0, one launch (start us, length us, event | category | flops | bytes accessed | tf_op | source)
XLA Modules:
  0.0 105.6 jit_solution(5868463281145894290)
XLA Ops:
  0.0 103.9 %shard_map.154 = bf16[64,2048]{1,0:T(8,128)(2,1)} custom-call(f32[4,256]{1,0:T(4,128)} %bitcast.12, bf16[256,512]{1,0:T(8,128)(2,1)} %k_hbm.1, f32[2,256,128]{2,1,0:T(8,128)} %constant.4.clone.near_hbm, f32[64,128]{1,0:T(8,128)} %constant.5.clone.base_hbm, bf16[256,512]{1,0:T(8,128)(2,1)} %v_hbm.1, bf16[256,512]{1,0:T(8,128)(2,1)} %q_hbm.1, ...), custom_call_target="tpu_custom_call" | custom-call | tf_op jit(solution)/shard_map/pallas_call | solution.py:868
  103.9 1.7 %copy.18 = bf16[64,2048]{1,0:T(8,128)(2,1)} copy(bf16[64,2048]{1,0:T(8,128)(2,1)} %shard_map.154) | data formatting | bytes 524288

commit v6 on v5

--- a/solution.py
+++ b/solution.py
@@ -159,18 +159,18 @@
 (
     UP_A, UP_B, DOWN_A, DOWN_B, X_A2, Y_B2, Y_A3, Y_A4, X_B3, X_B4, C_A, C_B, C_P, Y_A, X_B, X_A, Y_B, R_UP_A, R_UP_B,
     TOTAL, CHAIN, ACROSS, MIX_C, MIX_Y, S_X2, S_Y2, S_Y3, S_X3, S_Y4, S_X4, S_UP, S_DOWN, S_CORE,
-    T_UP, T_DOWN, T_Y1, T_X1, T_X2, T_Y2, R_DOWN_A, R_DOWN_B,
-) = range(41)
+    T_UP, T_DOWN, T_Y1, T_X1, T_X2, T_Y2, R_DOWN_A, R_DOWN_B, TOTAL_ON,
+) = range(42)
 
 
 def layer_kernel(
     planes, logs_hbm, k_hbm, near_hbm, base_hbm, v_hbm, q_hbm, gate_hbm, gain_hbm, routes_hbm, shares_hbm,
-    residual_hbm, ffn_gain_hbm, wo_hbm, wg_hbm, wu_hbm, wd_hbm, out,
+    residual_hbm, ffn_gain_hbm, wo_hbm, wg_hbm, wu_hbm, wd_hbm, out_hbm,
     logs, k_ref, near_table, base_table, v_ref, q_ref, gate_ref, head_gain, routes, route_weights,
     residual, ffn_gain, wo, wg, wu, wd, rotary, turned_k, ret, qdec, state, cum_col, cum_row, total_own, total_x, carry_in, carry_out,
     side_out, side_in, hidden, blend, from_core, held, from_y, upd,
     share_in, g0, g1, gs, pm, pr, a0, a1, r10, r11, b0, b1, r20, r21, d0, d1, low_up, low_down, high_up, high_down,
-    tot, tot_up, tot_down, home, home_in, pair, pair_in,
+    tot, tot_up, tot_down, home, home_in, pair, pair_in, total_prev, out,
     ssem, rsem, wsem,
 ):
     sp, tp = lax.axis_index("sp"), lax.axis_index("tp")
@@ -234,6 +234,7 @@
     def left(kind, n, src):
         move(kind, n, src, src, to_core).wait_send()
 
+    takes = (x == 0) & (z > 0)
     loads = [
         pltpu.make_async_copy(far, near, wsem.at[i])
         for i, (far, near) in enumerate(
@@ -251,6 +252,13 @@
     for device in [to_core, to_y, to_x] + [to_z(i) for i in range(1, planes)]:
         pl.semaphore_signal(barrier, inc=1, device_id=device, device_id_type=pl.DeviceIdType.MESH)
 
+
+    @pl.when(takes)
+    def _():
+        pl.semaphore_signal(
+            barrier, inc=1, device_id={"sp": z * 2 - 1, "tp": tp}, device_id_type=pl.DeviceIdType.MESH
+        )
+
     length = q_ref.shape[0]
     dim = HEAD_DIM
     heads = q_ref.shape[1] // dim
@@ -269,8 +277,14 @@
         ones, log_rows, (((1,), (1,)), ((), ())), precision=highest, preferred_element_type=f32
     )
     total_own[...] = jnp.broadcast_to(cum_row[:, length - 1 :], (8, dim))
-    pl.semaphore_wait(barrier, 2 + planes)
+    gives = (x == 1) & (z + 1 < planes)
+    pl.semaphore_wait(barrier, 2 + planes + jnp.where(gives, 1, 0))
     send(TOTAL, 0, total_own, total_x, to_x)
+
+    @pl.when(gives)
+    def _():
+        send(TOTAL_ON, 0, total_own, total_prev, {"sp": (z + 1) * 2, "tp": tp})
+
 
     loads[2].wait()
     loads[3].wait()
@@ -290,19 +304,31 @@
 
     left_side = x == 0
 
-    def pass_state(e):
+    def incoming(e):
+        return jnp.where(takes, jnp.exp(total_prev[e // cuts : e // cuts + 1, :]), 1.0) * carry_in[e].astype(f32)
+
+    def pass_state(e, first):
         h = e // cuts
-        own_total, x_total = total_own[h : h + 1, :], total_x[h : h + 1, :]
-        before = carry_in[e].astype(f32)
+        if first:
+            grown = state[e].astype(bf16)
+            before = jnp.zeros((depth, dim), bf16)
+        else:
+            near = incoming(e)
+            span = total_own[h : h + 1, :] + jnp.where(left_side, 0.0, total_x[h : h + 1, :])
+            grown = (jnp.exp(span) * near + state[e]).astype(bf16)
+            before = near.astype(bf16)
+        carry_out[e] = grown
+        side_out[e] = jnp.where(left_side, grown, before)
 
         @pl.when(z + 1 < planes)
         def _():
-            fresh = jnp.where(left_side, jnp.exp(x_total), 1.0) * state[e]
-            carry_out[e] = (jnp.exp(own_total + x_total) * before + fresh).astype(bf16)
             send(CHAIN, e, carry_out.at[e], carry_in.at[e], at_plane(z + 1))
 
-        side_out[e] = jnp.where(left_side, jnp.exp(own_total) * before + state[e], before).astype(bf16)
         send(ACROSS, e, side_out.at[e], side_in.at[e], to_x)
+
+    @pl.when(jnp.logical_not(takes))
+    def _():
+        total_prev[...] = jnp.zeros_like(total_prev)
 
     @pl.when(z == 0)
     def _():
@@ -331,10 +357,8 @@
 
         @pl.when(z == 0)
         def _():
-            if h == 0:
-                arrived(TOTAL, 0, total_x)
             for e in range(cuts * h, cuts * (h + 1)):
-                pass_state(e)
+                pass_state(e, True)
 
     def attend(h, carry):
         lanes = pl.ds(pl.multiple_of(h * dim, dim), dim)
@@ -353,16 +377,18 @@
     loads[5].wait()
     lax.fori_loop(0, early, attend, 0)
 
-    @pl.when(z > 0)
+    arrived(TOTAL, 0, total_x)
+
+    @pl.when(takes)
     def _():
-        arrived(TOTAL, 0, total_x)
+        arrived(TOTAL_ON, 0, total_prev)
 
     for e in range(cuts * heads):
 
         @pl.when(z > 0)
         def _():
             arrived(CHAIN, e, carry_in.at[e])
-            pass_state(e)
+            pass_state(e, False)
 
     lax.fori_loop(early, heads, attend, 0)
 
@@ -375,6 +401,7 @@
         for e in range(cuts * h, cuts * (h + 1)):
             arrived(ACROSS, e, side_in.at[e])
         factor = jnp.where(left_side, 1.0, jnp.exp(total_x[h : h + 1, :]))
+        factor = factor * jnp.where(takes, jnp.exp(total_prev[h : h + 1, :]), 1.0)
         before = carry_in[blocks].reshape(dim, dim).astype(f32)
         entering = (factor * before + side_in[blocks].reshape(dim, dim).astype(f32)).astype(bf16)
         retained = ret[:, lanes] + jnp.dot(qdec[:, lanes], entering, preferred_element_type=f32)
@@ -723,6 +750,7 @@
     lax.fori_loop(0, items + lag + 2, tick, 0)
     arrived(T_X2, 0, pair_in.at[0])
     arrived(T_Y2, 0, pair_in.at[1])
+    writes = []
     for r in range(2):
         n, part = 2 * z + r, pl.ds(r * rows, rows)
         low = upd[part, :half] + d0[n].astype(f32)
@@ -746,6 +774,9 @@
         out[part, 2 * half :] = (
             upd[part, 2 * half :] + kept.astype(f32) + pair_in[r].astype(f32)
         ).astype(bf16)
+        write = pltpu.make_async_copy(out.at[part], out_hbm.at[part], wsem.at[len(loads) + r])
+        write.start()
+        writes.append(write)
 
     left(T_Y1, 0, home.at[0, 1 - y])
     left(T_X1, 0, home.at[1, 1 - x])
@@ -812,6 +843,11 @@
 
     lax.fori_loop(0, planes, drain_side, 0)
     left(TOTAL, 0, total_own)
+
+    @pl.when(gives)
+    def _():
+        left(TOTAL_ON, 0, total_own)
+
     for e in range(cuts * heads):
         left(ACROSS, e, side_out.at[e])
 
@@ -822,6 +858,8 @@
     for j in range(pieces):
         left(MIX_C, j, blend.at[j, 1 - c])
         left(MIX_Y, j, held.at[j])
+    for write in writes:
+        write.wait()
 
 
 def rope_tables(length, spans):
@@ -869,7 +907,7 @@
         functools.partial(layer_kernel, planes),
         out_shape=jax.ShapeDtypeStruct((rows_all, width), bf16),
         in_specs=[far] * len(operands),
-        out_specs=whole,
+        out_specs=far,
         scratch_shapes=[
             *[pltpu.VMEM(operand.shape, operand.dtype) for operand in operands],
             pltpu.VMEM((2, length, HEAD_DIM), f32),
@@ -918,9 +956,11 @@
             pltpu.VMEM((2, 2, rows, wide_t), bf16),
             pltpu.VMEM((2, 2, rows, wide_t), bf16),
             pltpu.VMEM((2, rows, wide_t), bf16),
-            pltpu.SemaphoreType.DMA((41, max(items, 2 * heads, pieces))),
-            pltpu.SemaphoreType.DMA((41, max(items, 2 * heads, pieces))),
-            pltpu.SemaphoreType.DMA((len(operands),)),
+            pltpu.VMEM((8, HEAD_DIM), f32),
+            pltpu.VMEM((rows_all, width), bf16),
+            pltpu.SemaphoreType.DMA((42, max(items, 2 * heads, pieces))),
+            pltpu.SemaphoreType.DMA((42, max(items, 2 * heads, pieces))),
+            pltpu.SemaphoreType.DMA((len(operands) + 2,)),
         ],
         compiler_params=pltpu.CompilerParams(
             collective_id=0, has_side_effects=True, vmem_limit_bytes=63 * 1024 * 1024

time: 106 us -> 104 us (0.981)
  Pallas kernels: 104 us -> 102 us
    pallas_call x1, Pallas kernels: 104 us -> 102 us  [fused_layer(): pl.pallas_call(functools.partial(layer_kernel, planes), out_shape=jax.Sha...]
where the time goes in v6:
time: 104 us
  Pallas kernels  102 us (98%)
  local copies, waits for them, and re-layouts  1.67 us (2%)
    pallas_call x1, Pallas kernels, fused_layer(): pl.pallas_call(functools.partial(layer_kernel, planes), out_shape=jax.Sha...  102 us

profile of v6, /device:TPU:0, one launch (start us, length us, event | category | flops | bytes accessed | tf_op | source)
XLA Modules:
  0.0 103.5 jit_solution(13394417119054530115)
XLA Ops:
  0.0 101.9 %shard_map.154 = bf16[64,2048]{1,0:T(8,128)(2,1)} custom-call(f32[4,256]{1,0:T(4,128)} %bitcast.12, bf16[256,512]{1,0:T(8,128)(2,1)} %k_hbm.1, f32[2,256,128]{2,1,0:T(8,128)} %constant.4.clone.near_hbm, f32[64,128]{1,0:T(8,128)} %constant.5.clone.base_hbm, bf16[256,512]{1,0:T(8,128)(2,1)} %v_hbm.1, bf16[256,512]{1,0:T(8,128)(2,1)} %q_hbm.1, ...), custom_call_target="tpu_custom_call" | custom-call | tf_op jit(solution)/shard_map/pallas_call | solution.py:906
  101.9 1.7 %copy.18 = bf16[64,2048]{1,0:T(8,128)(2,1)} copy(bf16[64,2048]{1,0:T(8,128)(2,1)} %shard_map.154) | data formatting | bytes 524288

commit v7 on v6

--- a/solution.py
+++ b/solution.py
@@ -277,15 +277,6 @@
         ones, log_rows, (((1,), (1,)), ((), ())), precision=highest, preferred_element_type=f32
     )
     total_own[...] = jnp.broadcast_to(cum_row[:, length - 1 :], (8, dim))
-    gives = (x == 1) & (z + 1 < planes)
-    pl.semaphore_wait(barrier, 2 + planes + jnp.where(gives, 1, 0))
-    send(TOTAL, 0, total_own, total_x, to_x)
-
-    @pl.when(gives)
-    def _():
-        send(TOTAL_ON, 0, total_own, total_prev, {"sp": (z + 1) * 2, "tp": tp})
-
-
     loads[2].wait()
     loads[3].wait()
     base = base_table[pl.ds(sp * 8, 8), :]
@@ -354,6 +345,16 @@
         state[cuts * h : cuts * (h + 1)] = lax.dot_general(
             tailed, v_ref[:, lanes], (((0,), (0,)), ((), ())), preferred_element_type=f32
         ).reshape(cuts, depth, dim)
+
+        if h == 0:
+            gives = (x == 1) & (z + 1 < planes)
+            pl.semaphore_wait(barrier, 2 + planes + jnp.where(gives, 1, 0))
+            send(TOTAL, 0, total_own, total_x, to_x)
+
+            @pl.when(gives)
+            def _():
+                send(TOTAL_ON, 0, total_own, total_prev, {"sp": (z + 1) * 2, "tp": tp})
+
 
         @pl.when(z == 0)
         def _():
@@ -557,14 +558,14 @@
         def _():
             for up, _, acc, got_up, _ in chains:
                 arrived(up, n, got_up.at[n])
-                acc[n] = (acc[n].astype(f32) + got_up[n].astype(f32)).astype(bf16)
+                acc[n] = acc[n] + got_up[n]
                 send(up, n, acc.at[n], got_up.at[n], at_plane(z + 1))
 
         @pl.when((n // 2 < z) & (z < planes - 1))
         def _():
             for _, down, acc, _, got_down in chains:
                 arrived(down, n, got_down.at[n])
-                acc[n] = (acc[n].astype(f32) + got_down[n].astype(f32)).astype(bf16)
+                acc[n] = acc[n] + got_down[n]
                 send(down, n, acc.at[n], got_down.at[n], at_plane(z - 1))
 
     def tick(t, carry):
@@ -669,7 +670,7 @@
             arrived(C_P, n, pr.at[n])
             for q in range(4):
                 part = pl.ds(q * rows, rows)
-                total = (pm[n, c, part, :].astype(f32) + pr[n, part, :].astype(f32)).astype(bf16)
+                total = pm[n, c, part, :] + pr[n, part, :]
                 a0[n, q % 2, q // 2] = total[:, :half]
                 a1[n, q // 2, q % 2] = total[:, half : 2 * half]
                 tot[n, q] = total[:, 2 * half :]
@@ -681,19 +682,19 @@
         def _():
             n = item_of(step_of(t - lag - 1))
             arrived(Y_A, n, r10.at[n])
-            b0[n] = (a0[n, y].astype(f32) + r10[n].astype(f32)).astype(bf16)
+            b0[n] = a0[n, y] + r10[n]
             send(X_A, n, b0.at[n, 1 - x], r20.at[n], to_x)
             arrived(X_B, n, r11.at[n])
-            b1[n] = (a1[n, x].astype(f32) + r11[n].astype(f32)).astype(bf16)
+            b1[n] = a1[n, x] + r11[n]
             send(Y_B, n, b1.at[n, 1 - y], r21.at[n], to_y)
 
         @pl.when(has_turn(t - lag - 2))
         def _():
             n = item_of(step_of(t - lag - 2))
             arrived(X_A, n, r20.at[n])
-            d0[n] = (b0[n, x].astype(f32) + r20[n].astype(f32)).astype(bf16)
+            d0[n] = b0[n, x] + r20[n]
             arrived(Y_B, n, r21.at[n])
-            d1[n] = (b1[n, y].astype(f32) + r21[n].astype(f32)).astype(bf16)
+            d1[n] = b1[n, y] + r21[n]
             start_chain(n, main_chains)
 
         u = t - lag

time: 104 us -> 103 us (level)
  no operation moved by 1% of the time
where the time goes in v7:
time: 103 us
  Pallas kernels  101 us (98%)
  local copies, waits for them, and re-layouts  1.67 us (2%)
    pallas_call x1, Pallas kernels, fused_layer(): pl.pallas_call(functools.partial(layer_kernel, planes), out_shape=jax.Sha...  101 us

profile of v7, /device:TPU:0, one launch (start us, length us, event | category | flops | bytes accessed | tf_op | source)
XLA Modules:
  0.0 103.0 jit_solution(14492104319730511969)
XLA Ops:
  0.0 101.3 %shard_map.154 = bf16[64,2048]{1,0:T(8,128)(2,1)} custom-call(f32[4,256]{1,0:T(4,128)} %bitcast.12, bf16[256,512]{1,0:T(8,128)(2,1)} %k_hbm.1, f32[2,256,128]{2,1,0:T(8,128)} %constant.4.clone.near_hbm, f32[64,128]{1,0:T(8,128)} %constant.5.clone.base_hbm, bf16[256,512]{1,0:T(8,128)(2,1)} %v_hbm.1, bf16[256,512]{1,0:T(8,128)(2,1)} %q_hbm.1, ...), custom_call_target="tpu_custom_call" | custom-call | tf_op jit(solution)/shard_map/pallas_call | solution.py:907
  101.3 1.7 %copy.18 = bf16[64,2048]{1,0:T(8,128)(2,1)} copy(bf16[64,2048]{1,0:T(8,128)(2,1)} %shard_map.154) | data formatting | bytes 524288
